TPU v7x, 256 devices: a whole 4x4x8 slice. The times are simulated.
256 devices in a mesh: sp: 32 (over z, y), tp: 8 (over x, core).
Axes of the slice: x: 4, y: 4, z: 8, core: 2. Of those that a mesh axis runs over, the one named last changes fastest.
Arguments:
- prompt: bfloat16 [4, 6144, 4096], P(None, 'sp'), may hold values from -6 to 6
- forget_weight: bfloat16 [4096, 2048], P(None, 'tp'), may hold values from -0.09375 to 0.09375
- value_weight: bfloat16 [4096, 2048], P(None, 'tp'), may hold values from -1.5 to 1.5
- lower_bound: float32 [2048], P('tp'), may hold values from 0.9 to 0.99991862
- extra_decay: float32 [4, 6144, 2048], P(None, 'sp', 'tp'), may hold values from -1.40113932 to 0
- new_token: bfloat16 [4, 4096], P(None, 'tp'), may hold values from -6 to 6
- new_query: bfloat16 [4, 2048], P(None, 'tp'), may hold values from -6 to 6
- read_gain: float32 [128], replicated, may hold values from 0.1 to 1.9
Outputs:
- state_cache: bfloat16 [128, 16, 4, 128], P('sp', 'tp')
- first_read: bfloat16 [4, 2048], P(None, 'tp')
All inputs are finite; a program needn't handle non-finite values.
Results may differ from a plain program's by a relative error of at most 0.0019.
The roundings to bfloat16 on the way count: a program that leaves them out, or rounds other values in their place, can miss the bound.
Values may be sent and summed in bfloat16 or wider, within the bound.
No kernel may reach another device: no remote copies, remote signals or barrier semaphores. Data moves between devices by JAX's collectives and lax.ppermute only.
A program may use at most 64 MiB of HBM per device.

v0:
```python
import jax
import jax.numpy as jnp
from jax import lax
from jax.sharding import PartitionSpec as P

HD = 128


def from_everyone(array, axis):
    devices = lax.axis_size(axis)
    return lax.all_to_all(
        jnp.broadcast_to(array[None], (devices, *array.shape)), axis, 0, 0, tiled=True
    )


def joined_by_halves(pieces, combine):
    while len(jax.tree.leaves(pieces)[0]) > 1:
        pieces = jax.vmap(combine)(*(pieces[side::2] for side in (0, 1)))
    return pieces[0]


def carried_in(array, axis, combine, identity):
    devices, index = (lax.axis_size(axis), lax.axis_index(axis))
    passed = jnp.arange(devices) > index

    def kept(part, zero, own):
        part = jnp.where(
            passed.reshape(-1, *(1 for _ in own.shape)), part, jnp.asarray(zero, own.dtype)
        )
        return part[::-1]

    pieces = from_everyone(array, axis)
    return joined_by_halves(kept(pieces, identity, array), combine)


def laid_out(pieces, dim):
    shape = list(pieces.shape[1:])
    shape[dim] *= pieces.shape[0]
    return jnp.moveaxis(pieces, 0, dim).reshape(shape)


def collect(array, axis, dim):
    pieces = from_everyone(array, axis)
    return laid_out(pieces, dim)


def add_terms(earlier, latter):
    return earlier + latter


def read_share(state_rows, decay_rows, key_share, query_rows, new_value):
    updated = jnp.exp(decay_rows)[..., None] * state_rows + key_share[..., None] * new_value[None]
    return jnp.sum(query_rows[..., None] * updated, axis=0)


def local(
    prompt, forget_weight, value_weight, lower_bound, extra_decay, new_token, new_query, read_gain
):
    seq_count = prompt.shape[0]
    span_len = prompt.shape[1]
    width_dev = forget_weight.shape[1]
    head_count = width_dev // HD
    log_lower = jnp.log(lower_bound)
    log_upper = jnp.log1p(-lower_bound)
    opening = 1.0 - lower_bound
    forget_pre = jnp.einsum(
        "std,dw->stw", prompt, forget_weight, preferred_element_type=jnp.float32
    ).astype(jnp.bfloat16)
    values = jnp.einsum(
        "std,dw->stw", prompt, value_weight, preferred_element_type=jnp.float32
    ).astype(jnp.bfloat16)
    forget_wide = lax.optimization_barrier(forget_pre).astype(jnp.float32)
    log_forget = jnp.logaddexp(log_lower, log_upper + jax.nn.log_sigmoid(forget_wide)) + extra_decay
    key_rows = opening * jax.nn.sigmoid(-forget_wide)
    running = jnp.cumsum(log_forget, axis=1)
    totals = running[:, -1]
    weighted = (key_rows * jnp.exp(totals[:, None] - running)).astype(jnp.bfloat16)
    weighted = weighted.reshape(seq_count, span_len, head_count, HD)
    value_rows = values.reshape(seq_count, span_len, head_count, HD)
    later_sum = carried_in(totals, "sp", add_terms, jnp.zeros_like(totals))
    end_scale = jnp.exp(later_sum).reshape(seq_count, head_count, HD).transpose(2, 1, 0)
    whole_token = collect(new_token, "tp", 1)
    new_forget = lax.optimization_barrier(
        jnp.dot(whole_token, forget_weight, preferred_element_type=jnp.float32).astype(jnp.bfloat16)
    ).astype(jnp.float32)
    new_value = lax.optimization_barrier(
        jnp.dot(whole_token, value_weight, preferred_element_type=jnp.float32).astype(jnp.bfloat16)
    ).astype(jnp.float32)
    new_log = jnp.logaddexp(log_lower, log_upper + jax.nn.log_sigmoid(new_forget))
    new_key = opening * jax.nn.sigmoid(-new_forget)
    query_act = jax.nn.silu(new_query.astype(jnp.float32))
    decay_cols = new_log.reshape(seq_count, head_count, HD).transpose(2, 1, 0)
    key_cols = new_key.reshape(seq_count, head_count, HD).transpose(2, 1, 0)
    query_cols = query_act.reshape(seq_count, head_count, HD).transpose(2, 1, 0)
    value_cols = new_value.reshape(seq_count, head_count, HD).transpose(1, 0, 2)
    row_share = HD // lax.axis_size("sp")
    first_own = lax.axis_index("sp") * row_share
    block_state = jnp.einsum(
        "sthd,sthe->dhse", weighted, value_rows, preferred_element_type=jnp.float32
    )
    whole_state = lax.psum(block_state * end_scale[..., None], "sp")
    state_cache = lax.dynamic_slice_in_dim(whole_state, first_own, row_share, 0).astype(
        jnp.bfloat16
    )
    raw_read = read_share(whole_state, decay_cols, key_cols, query_cols, value_cols)
    raw_read = raw_read.transpose(1, 0, 2)
    normed = (
        raw_read
        * lax.rsqrt(jnp.mean(raw_read * raw_read, axis=-1, keepdims=True) + 1e-06)
        * read_gain
    )
    first_read = normed.reshape(seq_count, width_dev).astype(jnp.bfloat16)
    return (state_cache, first_read)


def solution(mesh):
    return jax.shard_map(
        local,
        mesh=mesh,
        in_specs=(
            P(None, "sp", None),
            P(None, "tp"),
            P(None, "tp"),
            P("tp"),
            P(None, "sp", "tp"),
            P(None, "tp"),
            P(None, "tp"),
            P(),
        ),
        out_specs=(P("sp", "tp", None, None), P(None, "tp")),
        check_vma=False,
    )
```

profile of v0, /device:TPU:2, one launch (start us, length us, event | category | flops | bytes accessed | tf_op | source)
XLA Modules:
  0.0 208.9 jit_solution(13136522853903477790)
XLA Ops:
  7.2 0.0 copy-start
  7.2 1.4 broadcast_in_dim.21
  8.6 5.5 %all-to-all-start.1 = ((bf16[8,4,512]{2,1,0:T(4,128)(2,1)}), bf16[8,4,512]{2,1,0:T(4,128)(2,1)S(1)}, u32[]{:S(2)}, u32[]{:S(2)}) async-start(bf16[8,4,512]{2,1,0:T(4,128)(2,1)} %broadcast_in_dim.21), calls=%async_computation.1 | async-start | bytes 65536 | tf_op jit(solution)/shard_map/all_to_all | solution.py:11
  14.1 0.7 broadcast_subtract_fusion
  14.8 0.0 copy-done
  14.8 0.0 copy-start.2
  14.8 4.6 %fusion.7 = bf16[4,192,256]{2,1,0:T(8,128)(2,1)S(1)} fusion(bf16[4,192,4096]{2,1,0:T(8,128)(2,1)} %param.8, bf16[4096,256]{1,0:T(8,128)(2,1)S(1)} %copy-done), kind=kOutput, calls=%fused_computation.6 | convolution fusion | flops 1610809344 | bytes 8781824 | tf_op jit(solution)/shard_map/std,dw->stw/dot_general | solution.py:66
  19.5 0.0 copy-start.3
  19.5 0.0 copy-done.2
  19.5 1.0 add_bitcast_fusion
  20.5 0.1 pad.3
  20.6 0.0 copy-done.3
  20.6 0.8 fusion.14
  21.5 1.3 broadcast_add_fusion
  22.8 0.0 copy-start.1
  22.8 6.0 %fusion.11 = bf16[4,24,2,8,128]{4,3,2,1,0:T(8,128)(2,1)} fusion(bf16[4,192,4096]{2,1,0:T(8,128)(2,1)} %param.8, bf16[4096,256]{1,0:T(8,128)(2,1)} %param.10), kind=kOutput, calls=%fused_computation.9 | convolution fusion | flops 1610809344 | bytes 8781824 | tf_op jit(solution)/shard_map/std,dw->stw/dot_general | solution.py:69
  28.9 0.0 copy-done.1
  28.9 0.1 copy.20
  29.0 0.0 all-to-all-done.1
  29.0 0.7 broadcast_in_dim.19
  29.7 10.8 %all-to-all-start = ((f32[32,4,256]{2,1,0:T(4,128)}), f32[32,4,256]{2,1,0:T(4,128)S(1)}, u32[]{:S(2)}, u32[]{:S(2)}) async-start(f32[32,4,256]{2,1,0:T(4,128)} %broadcast_in_dim.19), calls=%async_computation | async-start | bytes 262144 | tf_op jit(solution)/shard_map/all_to_all | solution.py:11
  40.5 0.0 all-reduce.3.cloned.1.call-start
  40.6 0.4 convolution_convert_fusion.1
  40.9 10.3 %all-to-all-done = f32[32,4,256]{2,1,0:T(4,128)S(1)} async-done(((f32[32,4,256]{2,1,0:T(4,128)}), f32[32,4,256]{2,1,0:T(4,128)S(1)}, u32[]{:S(2)}, u32[]{:S(2)}) %all-to-all-start) | async-done | bytes 131104 | tf_op jit(solution)/shard_map/all_to_all | solution.py:11
  51.3 0.1 broadcast_select_fusion
  51.5 2.5 %fusion.10 = f32[128,2,4,128]{0,3,2,1:T(8,128)} fusion(bf16[4,24,2,8,128]{4,3,2,1,0:T(8,128)(2,1)} %fusion.11, f32[128,2,4]{0,2,1:T(4,128)S(1)} %fusion.51, f32[4,256,256]{2,1,0:T(8,128)S(1)} %bitcast.84, f32[4,256]{1,0:T(4,128)S(1)} %bitcast.88, bf16[4,192,256]{2,1,0:T(8,128)(2,1)} %copy-done.3, f32[256]{0:T(256)S(1)} %get-tuple-element.10), kind=kOutput, calls=%fused_computation.8 | convolution fusion | flops 51838976 | bytes 2106368 | tf_op jit(solution)/shard_map/sthd,sthe->dhse/dot_general | solution.py:98
  53.9 0.0 copy-start.4
  53.9 0.0 copy-start.5
  53.9 0.0 all-reduce.3.cloned.1.call-update
  54.0 2.0 convolution_convert_fusion
  56.0 0.0 copy-done.4
  56.0 142.0 %all-reduce.3.cloned.1.call-done = f32[128,2,4,128]{0,3,2,1:T(8,128)} async-done(((f32[128,2,4,128]{0,3,2,1:T(8,128)}), f32[128,2,4,128]{0,3,2,1:T(8,128)}) %all-reduce.3.cloned.1.call-update) | async-done | bytes 524304 | tf_op jit(solution)/shard_map/psum | solution.py:101
  198.0 1.4 multiply_reduce_fusion
  199.4 0.1 fusion.52
  199.5 1.2 dynamic-slice_convert_fusion
  200.7 0.7 copy.27
  201.4 0.0 copy-done.5
  201.4 0.7 fusion.55
  (15 shorter events, 0.2 us)
Async XLA Ops:
  7.2 7.6 %copy-start = (bf16[4096,256]{1,0:T(8,128)(2,1)S(1)}, bf16[4096,256]{1,0:T(8,128)(2,1)}, u32[]{:S(2)}) copy-start(bf16[4096,256]{1,0:T(8,128)(2,1)} %param.9) | copy-start | bytes 6291460
  8.6 20.4 %all-to-all-start.1 = ((bf16[8,4,512]{2,1,0:T(4,128)(2,1)}), bf16[8,4,512]{2,1,0:T(4,128)(2,1)S(1)}, u32[]{:S(2)}, u32[]{:S(2)}) async-start(bf16[8,4,512]{2,1,0:T(4,128)(2,1)} %broadcast_in_dim.21), calls=%async_computation.1 | async-start | bytes 65536 | tf_op jit(solution)/shard_map/all_to_all | solution.py:11
  14.8 4.7 %copy-start.2 = (f32[4,192,256]{2,1,0:T(8,128)S(1)}, f32[4,192,256]{2,1,0:T(8,128)}, u32[]{:S(2)}) copy-start(f32[4,192,256]{2,1,0:T(8,128)} %param.12) | copy-start | bytes 2359300
  19.5 1.1 copy-start.3
  22.8 6.0 %copy-start.1 = (f32[4,256,2,128]{1,2,3,0:T(2,128)S(1)}, f32[4,256,2,128]{1,2,3,0:T(2,128)}, u32[]{:S(2)}) copy-start(f32[4,256,2,128]{1,2,3,0:T(2,128)} %broadcast_add_fusion) | copy-start | bytes 3145732
  29.7 21.6 %all-to-all-start = ((f32[32,4,256]{2,1,0:T(4,128)}), f32[32,4,256]{2,1,0:T(4,128)S(1)}, u32[]{:S(2)}, u32[]{:S(2)}) async-start(f32[32,4,256]{2,1,0:T(4,128)} %broadcast_in_dim.19), calls=%async_computation | async-start | bytes 262144 | tf_op jit(solution)/shard_map/all_to_all | solution.py:11
  40.5 157.5 %all-reduce.3.cloned.1.call-start = ((), (), s32[]{:S(2)}) async-start(), calls=%async_computation.2 | async-start | bytes 1048576 | tf_op jit(solution)/shard_map/psum | solution.py:101
  53.9 2.0 copy-start.4
  53.9 147.5 %copy-start.5 = (f32[128]{0:T(128)S(1)}, f32[128]{0:T(128)}, u32[]{:S(2)}) copy-start(f32[128]{0:T(128)} %param.15) | copy-start | bytes 1540
Sparse Core Ops, SparseCore 0:
  54.1 143.8 all-reduce.2
where the time goes:
time: 209 us
  waiting for transfers between devices  152 us (73%)
  starting transfers between devices  16.4 us (8%)
  matrix products  15.5 us (7%)
  between operations  14.2 us (7%)
  other arithmetic  6.27 us (3%)
  local copies, waits for them, and re-layouts  4.27 us (2%)
    psum x1, waiting for transfers between devices, local(): whole_state = lax.psum(block_state * end_scale[..., None], 'sp')  142 us
    all_to_all x2, starting transfers between devices, from_everyone(): lax.all_to_all(jnp.broadcast_to(array[None], (devices, *array.shape)), ax...  16.3 us
    all_to_all x2, waiting for transfers between devices, from_everyone(): lax.all_to_all(jnp.broadcast_to(array[None], (devices, *array.shape)), ax...  10.3 us
    dot_general x1, matrix products, local(): jnp.einsum('std,dw->stw', prompt, value_weight, preferred_element_type=jn...  6.04 us
    dot_general x1, matrix products, local(): jnp.einsum('std,dw->stw', prompt, forget_weight, preferred_element_type=j...  4.64 us
  transfers between devices with their start and end apart: 3, of which 2 were waited for; matrix products, arithmetic and copies ran while one was open for 8% of the time, Pallas kernels for 0%

commit v1 on v0

v1 whole, which is shorter than its diff:
```python
import jax
import jax.numpy as jnp
from jax import lax
from jax.sharding import PartitionSpec as P

HD = 128


def from_everyone(array, axis):
    devices = lax.axis_size(axis)
    return lax.all_to_all(
        jnp.broadcast_to(array[None], (devices, *array.shape)), axis, 0, 0, tiled=True
    )


def local(
    prompt, forget_weight, value_weight, lower_bound, extra_decay, new_token, new_query, read_gain
):
    seq_count, span_len, _ = prompt.shape
    width_dev = forget_weight.shape[1]
    head_count = width_dev // HD
    blocks = lax.axis_size("sp")
    row_share = HD // blocks
    rows = head_count * seq_count * row_share
    block = lax.axis_index("sp")
    log_lower = jnp.log(lower_bound)
    log_upper = jnp.log1p(-lower_bound)
    opening = 1.0 - lower_bound
    forget_pre = jnp.einsum(
        "std,dw->stw", prompt, forget_weight, preferred_element_type=jnp.float32
    ).astype(jnp.bfloat16)
    values = jnp.einsum(
        "std,dw->stw", prompt, value_weight, preferred_element_type=jnp.float32
    ).astype(jnp.bfloat16)
    forget_wide = lax.optimization_barrier(forget_pre).astype(jnp.float32)
    log_forget = jnp.logaddexp(log_lower, log_upper + jax.nn.log_sigmoid(forget_wide)) + extra_decay
    key_rows = opening * jax.nn.sigmoid(-forget_wide)
    running = jnp.cumsum(log_forget, axis=1)
    totals = running[:, -1]
    weighted = (key_rows * jnp.exp(totals[:, None] - running)).astype(jnp.bfloat16)
    weighted = weighted.reshape(seq_count, span_len, head_count, HD)
    value_rows = values.reshape(seq_count, span_len, head_count, HD)
    block_state = jnp.einsum(
        "sthd,sthe->hsde", weighted, value_rows, preferred_element_type=jnp.float32
    )
    sent = block_state.reshape(head_count, seq_count, blocks, row_share, HD)
    sent = sent.transpose(2, 0, 1, 3, 4).reshape(blocks, rows, HD)
    sent_totals = totals.reshape(seq_count, head_count, blocks, row_share)
    sent_totals = sent_totals.transpose(2, 1, 0, 3).reshape(blocks, 1, rows)
    sent_totals = jnp.pad(sent_totals, ((0, 0), (0, 0), (0, HD - rows)))
    got = lax.all_to_all(jnp.concatenate([sent, sent_totals], 1), "sp", 0, 0, tiled=True)
    got_totals = got[:, rows, :rows]
    later = jnp.arange(blocks)[:, None] < jnp.arange(blocks)[None, :]
    later_sum = jnp.sum(jnp.where(later[:, :, None], got_totals[None], 0.0), axis=1)
    final = jnp.sum(jnp.exp(later_sum)[..., None] * got[:, :rows], axis=0)
    final = final.reshape(head_count, seq_count, row_share, HD)
    state_cache = final.transpose(2, 0, 1, 3).astype(jnp.bfloat16)

    pieces = from_everyone(new_token, "tp")
    whole_token = pieces.transpose(1, 0, 2).reshape(seq_count, -1)
    new_forget = lax.optimization_barrier(
        jnp.dot(whole_token, forget_weight, preferred_element_type=jnp.float32).astype(jnp.bfloat16)
    ).astype(jnp.float32)
    new_value = lax.optimization_barrier(
        jnp.dot(whole_token, value_weight, preferred_element_type=jnp.float32).astype(jnp.bfloat16)
    ).astype(jnp.float32)
    new_log = jnp.logaddexp(log_lower, log_upper + jax.nn.log_sigmoid(new_forget))
    new_key = opening * jax.nn.sigmoid(-new_forget)
    query_act = jax.nn.silu(new_query.astype(jnp.float32))

    def own(array):
        parts = array.reshape(seq_count, head_count, blocks, row_share)
        return lax.dynamic_index_in_dim(parts, block, 2, keepdims=False).transpose(1, 0, 2)

    share = jnp.sum(own(query_act * jnp.exp(new_log))[..., None] * final, axis=2)
    shares = from_everyone(share.reshape(head_count * seq_count, HD), "sp")
    raw_read = jnp.sum(shares, axis=0).reshape(head_count, seq_count, HD).transpose(1, 0, 2)
    key_sum = jnp.sum((query_act * new_key).reshape(seq_count, head_count, HD), axis=-1)
    raw_read = raw_read + key_sum[..., None] * new_value.reshape(seq_count, head_count, HD)
    normed = (
        raw_read
        * lax.rsqrt(jnp.mean(raw_read * raw_read, axis=-1, keepdims=True) + 1e-06)
        * read_gain
    )
    first_read = normed.reshape(seq_count, width_dev).astype(jnp.bfloat16)
    return (state_cache, first_read)


def solution(mesh):
    return jax.shard_map(
        local,
        mesh=mesh,
        in_specs=(
            P(None, "sp", None),
            P(None, "tp"),
            P(None, "tp"),
            P("tp"),
            P(None, "sp", "tp"),
            P(None, "tp"),
            P(None, "tp"),
            P(),
        ),
        out_specs=(P("sp", "tp", None, None), P(None, "tp")),
        check_vma=False,
    )
```

time: 209 us -> 74.8 us (0.36)
  waiting for transfers between devices: 152 us -> 26.9 us
  between operations: 14.2 us -> 0.91 us
  starting transfers between devices: 16.4 us -> 21.3 us
  matrix products: 15.5 us -> 12.9 us
  local copies, waits for them, and re-layouts: 4.27 us -> 6.48 us
    psum x1 -> x0, waiting for transfers between devices: 142 us -> none  [local(): whole_state = lax.psum(block_state * end_scale[..., None], 'sp')]
    all_to_all x0 -> x1, waiting for transfers between devices: none -> 18.9 us  [local(): lax.all_to_all(jnp.concatenate([sent, sent_totals], 1), 'sp', 0, 0, tiled...]
    all_to_all x0 -> x1, starting transfers between devices: none -> 10.3 us  [local(): lax.all_to_all(jnp.concatenate([sent, sent_totals], 1), 'sp', 0, 0, tiled...]
    all_to_all x2, starting transfers between devices: 16.3 us -> 11 us  [from_everyone(): lax.all_to_all(jnp.broadcast_to(array[None], (devices, *array.shape)), ax...]
    all_to_all x2, waiting for transfers between devices: 10.3 us -> 8.04 us  [from_everyone(): lax.all_to_all(jnp.broadcast_to(array[None], (devices, *array.shape)), ax...]
  transfers between devices with their start and end apart: 3 -> 3, of which waited for: 2 -> 2; matrix products, arithmetic and copies ran while one was open for 8% -> 28% of each run, Pallas kernels for 0% -> 0%
where the time goes in v1:
time: 74.8 us; the launch traced here: 74.3 us
  waiting for transfers between devices  26.9 us (36%)
  starting transfers between devices  21.3 us (28%)
  matrix products  12.9 us (17%)
  local copies, waits for them, and re-layouts  6.48 us (9%)
  other arithmetic  5.74 us (8%)
  between operations  0.91 us (1%)
    all_to_all x1, waiting for transfers between devices, local(): lax.all_to_all(jnp.concatenate([sent, sent_totals], 1), 'sp', 0, 0, tiled...  18.9 us
    all_to_all x2, starting transfers between devices, from_everyone(): lax.all_to_all(jnp.broadcast_to(array[None], (devices, *array.shape)), ax...  11 us
    all_to_all x1, starting transfers between devices, local(): lax.all_to_all(jnp.concatenate([sent, sent_totals], 1), 'sp', 0, 0, tiled...  10.3 us
    all_to_all x2, waiting for transfers between devices, from_everyone(): lax.all_to_all(jnp.broadcast_to(array[None], (devices, *array.shape)), ax...  8.04 us
    dot_general x1, matrix products, local(): jnp.einsum('std,dw->stw', prompt, forget_weight, preferred_element_type=j...  4.65 us
    dot_general x1, matrix products, local(): jnp.einsum('std,dw->stw', prompt, value_weight, preferred_element_type=jn...  4.62 us
    broadcast_in_dim x2, local copies, waits for them, and re-layouts, from_everyone(): jnp.broadcast_to(array[None], (devices, *array.shape))  2.1 us
    dot_general x1, matrix products, local(): jnp.dot(whole_token, value_weight, preferred_element_type=jnp.float32)  1.99 us
  transfers between devices with their start and end apart: 3, of which 2 were waited for; matrix products, arithmetic and copies ran while one was open for 28% of the time, Pallas kernels for 0%

profile of v1, /device:TPU:2, one launch (start us, length us, event | category | flops | bytes accessed | tf_op | source)
XLA Modules:
  0.0 74.3 jit_solution(7973804270257246484)
XLA Ops:
  0.6 0.0 copy-start
  0.6 1.5 %broadcast_in_dim.32 = bf16[8,4,512]{2,1,0:T(4,128)(2,1)} broadcast(bf16[4,512]{1,0:T(4,128)(2,1)} %param.13), dimensions={1,2} | broadcast | bytes 36864 | tf_op jit(solution)/shard_map/broadcast_in_dim | solution.py:12
  2.1 6.0 %all-to-all-start.1 = ((bf16[8,4,512]{2,1,0:T(4,128)(2,1)}), bf16[8,4,512]{2,1,0:T(4,128)(2,1)}, u32[]{:S(2)}, u32[]{:S(2)}) async-start(bf16[8,4,512]{2,1,0:T(4,128)(2,1)} %broadcast_in_dim.32), calls=%async_computation.1 | async-start | bytes 65536 | tf_op jit(solution)/shard_map/all_to_all | solution.py:11
  8.1 1.2 %broadcast_subtract_fusion = (f32[256]{0:T(256)}, f32[256]{0:T(256)S(1)}, f32[256]{0:T(256)S(1)}) fusion(f32[256]{0:T(256)} %param.11), kind=kLoop, calls=%fused_computation.74 | loop fusion | flops 512 | bytes 4096 | tf_op jit(solution)/shard_map/sub | solution.py:28
  9.4 0.0 copy-done
  9.4 4.6 %fusion.4 = bf16[4,192,256]{2,1,0:T(8,128)(2,1)S(1)} fusion(bf16[4,192,4096]{2,1,0:T(8,128)(2,1)} %param.8, bf16[4096,256]{1,0:T(8,128)(2,1)S(1)} %copy-done), kind=kOutput, calls=%fused_computation.5 | convolution fusion | flops 1610809344 | bytes 8781824 | tf_op jit(solution)/shard_map/std,dw->stw/dot_general | solution.py:29
  14.1 0.0 copy-done.3
  14.1 0.0 copy-done.5
  14.1 0.0 copy-done.2
  14.1 1.0 %add_bitcast_fusion = f32[4,256,192]{1,2,0:T(8,128)S(1)} fusion(f32[4,192,256]{2,1,0:T(8,128)S(1)} %copy-done.2, bf16[4,192,256]{2,1,0:T(8,128)(2,1)S(1)} %fusion.4, f32[256]{0:T(256)S(1)} %get-tuple-element.15, f32[256]{0:T(256)S(1)} %get-tuple-element.16), kind=kLoop, calls=%fused_computation.28 | loop fusion | flops 3735552 | bytes 1968128 | tf_op jit(solution)/shard_map/transpose
  15.1 0.1 pad.7
  15.2 0.8 %fusion.13 = f32[4,256,2,128]{1,2,3,0:T(2,128)S(1)} fusion(f32[4,256,2,128]{1,3,2,0:T(8,128)S(1)} %bitcast.67), kind=kOutput, calls=%fused_computation.10 | output fusion | flops 33292288 | bytes 2097152 | tf_op jit(solution)/shard_map/reduce-window
  16.0 0.6 slice_bitcast_fusion
  16.6 0.7 reduce-window.9
  17.4 0.0 copy-start.1
  17.4 0.4 broadcast_add_fusion
  17.7 0.1 copy.39
  17.9 1.1 %copy-done.1 = bf16[4096,256]{1,0:T(8,128)(2,1)S(1)} copy-done((bf16[4096,256]{1,0:T(8,128)(2,1)S(1)}, bf16[4096,256]{1,0:T(8,128)(2,1)}, u32[]{:S(2)}) %copy-start.1) | copy-done | bytes 2097176
  19.0 4.6 %fusion.10 = bf16[4,24,2,8,128]{4,3,2,1,0:T(8,128)(2,1)S(1)} fusion(bf16[4,192,4096]{2,1,0:T(8,128)(2,1)} %param.8, bf16[4096,256]{1,0:T(8,128)(2,1)S(1)} %copy-done.1), kind=kOutput, calls=%fused_computation.7 | convolution fusion | flops 1610809344 | bytes 8781824 | tf_op jit(solution)/shard_map/std,dw->stw/dot_general | solution.py:32
  23.6 0.0 copy-done.7
  23.6 0.5 fusion.30
  24.1 0.1 copy.42
  24.2 0.1 reshape_squeeze.3
  24.3 0.1 copy.43
  24.5 0.1 copy.44
  24.5 0.1 select_maximum_fusion
  24.6 0.0 copy-start.8
  24.6 1.2 %copy.45 = f32[32,33,128]{2,1,0:T(8,128)} copy(f32[32,33,128]{2,0,1:T(8,128)S(1)} %select_maximum_fusion) | data formatting | bytes 1081344 | tf_op jit(solution)/shard_map/concatenate | solution.py:51
  25.8 0.0 all-to-all-done.1
  25.8 10.3 %all-to-all-start = ((f32[32,33,128]{2,1,0:T(8,128)}), f32[32,33,128]{2,1,0:T(8,128)S(1)}, u32[]{:S(2)}, u32[]{:S(2)}) async-start(f32[32,33,128]{2,1,0:T(8,128)} %copy.45), calls=%async_computation | async-start | bytes 1310720 | tf_op jit(solution)/shard_map/all_to_all | solution.py:51
  36.1 1.1 %convolution_convert_fusion.1 = bf16[4,256]{1,0:T(4,128)(2,1)S(1)} fusion(bf16[4,4096]{1,0:T(4,128)(2,1)} %bitcast.17, bf16[4096,256]{1,0:T(8,128)(2,1)S(1)} %copy-done), kind=kOutput, calls=%fused_computation.9 | convolution fusion | flops 8389632 | bytes 2131968 | tf_op jit(solution)/shard_map/dot_general | solution.py:62
  37.2 0.0 copy-done.4
  37.2 0.0 copy-done.6
  37.2 0.0 copy-start.9
  37.3 0.1 reshape.96
  37.5 0.1 reduce_sum.58
  37.6 0.1 copy.47
  37.7 18.9 %all-to-all-done = f32[32,33,128]{2,1,0:T(8,128)S(1)} async-done(((f32[32,33,128]{2,1,0:T(8,128)}), f32[32,33,128]{2,1,0:T(8,128)S(1)}, u32[]{:S(2)}, u32[]{:S(2)}) %all-to-all-start) | async-done | bytes 540704 | tf_op jit(solution)/shard_map/all_to_all | solution.py:51
  56.6 0.2 select_reduce_fusion
  56.8 0.2 fusion.29
  57.0 0.1 multiply_reduce_fusion
  57.1 0.7 broadcast_in_dim.34
  57.8 5.0 %all-to-all-start.2 = ((f32[32,8,128]{2,1,0:T(8,128)}), f32[32,8,128]{2,1,0:T(8,128)S(1)}, u32[]{:S(2)}, u32[]{:S(2)}) async-start(f32[32,8,128]{2,1,0:T(8,128)} %broadcast_in_dim.34), calls=%async_computation.2 | async-start | bytes 262144 | tf_op jit(solution)/shard_map/all_to_all | solution.py:11
  62.8 2.0 %convolution_convert_fusion = bf16[4,256]{1,0:T(4,128)(2,1)S(1)} fusion(bf16[4,4096]{1,0:T(4,128)(2,1)} %bitcast.17, bf16[4096,256]{1,0:T(8,128)(2,1)} %param.10), kind=kOutput, calls=%fused_computation.8 | convolution fusion | flops 8389632 | bytes 2131968 | tf_op jit(solution)/shard_map/dot_general | solution.py:65
  64.8 0.6 copy.49
  65.4 8.0 %all-to-all-done.2 = f32[32,8,128]{2,1,0:T(8,128)S(1)} async-done(((f32[32,8,128]{2,1,0:T(8,128)}), f32[32,8,128]{2,1,0:T(8,128)S(1)}, u32[]{:S(2)}, u32[]{:S(2)}) %all-to-all-start.2) | async-done | bytes 131104 | tf_op jit(solution)/shard_map/all_to_all | solution.py:11
  73.4 0.2 multiply_reduce_fusion.1
  73.6 0.7 fusion.51
  (20 shorter events, 0.2 us)
Async XLA Ops:
  0.6 8.8 %copy-start = (bf16[4096,256]{1,0:T(8,128)(2,1)S(1)}, bf16[4096,256]{1,0:T(8,128)(2,1)}, u32[]{:S(2)}) copy-start(bf16[4096,256]{1,0:T(8,128)(2,1)} %param.9) | copy-start | bytes 6291460
  2.1 23.7 %all-to-all-start.1 = ((bf16[8,4,512]{2,1,0:T(4,128)(2,1)}), bf16[8,4,512]{2,1,0:T(4,128)(2,1)}, u32[]{:S(2)}, u32[]{:S(2)}) async-start(bf16[8,4,512]{2,1,0:T(4,128)(2,1)} %broadcast_in_dim.32), calls=%async_computation.1 | async-start | bytes 65536 | tf_op jit(solution)/shard_map/all_to_all | solution.py:11
  9.4 4.7 %copy-start.3 = (f32[256]{0:T(256)}, f32[256]{0:T(256)S(1)}, u32[]{:S(2)}) copy-start(f32[256]{0:T(256)S(1)} %get-tuple-element.15) | copy-start | bytes 3076
  9.4 4.7 %copy-start.5 = (f32[256]{0:T(256)}, f32[256]{0:T(256)S(1)}, u32[]{:S(2)}) copy-start(f32[256]{0:T(256)S(1)} %get-tuple-element.16) | copy-start | bytes 3076
  9.4 4.7 %copy-start.2 = (f32[4,192,256]{2,1,0:T(8,128)S(1)}, f32[4,192,256]{2,1,0:T(8,128)}, u32[]{:S(2)}) copy-start(f32[4,192,256]{2,1,0:T(8,128)} %param.12) | copy-start | bytes 2359300
  17.4 1.6 %copy-start.1 = (bf16[4096,256]{1,0:T(8,128)(2,1)S(1)}, bf16[4096,256]{1,0:T(8,128)(2,1)}, u32[]{:S(2)}) copy-start(bf16[4096,256]{1,0:T(8,128)(2,1)} %param.10) | copy-start | bytes 6291460
  19.0 4.6 %copy-start.7 = (f32[256]{0:T(256)S(1)}, f32[256]{0:T(256)}, u32[]{:S(2)}) copy-start(f32[256]{0:T(256)} %get-tuple-element.14) | copy-start | bytes 3076
  24.6 12.6 %copy-start.4 = (f32[256]{0:T(256)S(1)}, f32[256]{0:T(256)}, u32[]{:S(2)}) copy-start(f32[256]{0:T(256)} %copy-done.3) | copy-start | bytes 3076
  24.6 12.6 %copy-start.6 = (f32[256]{0:T(256)S(1)}, f32[256]{0:T(256)}, u32[]{:S(2)}) copy-start(f32[256]{0:T(256)} %copy-done.5) | copy-start | bytes 3076
  24.6 12.6 %copy-start.8 = (bf16[4,256]{1,0:T(4,128)(2,1)S(1)}, bf16[4,256]{1,0:T(4,128)(2,1)}, u32[]{:S(2)}) copy-start(bf16[4,256]{1,0:T(4,128)(2,1)} %param.14) | copy-start | bytes 6148
  25.8 30.8 %all-to-all-start = ((f32[32,33,128]{2,1,0:T(8,128)}), f32[32,33,128]{2,1,0:T(8,128)S(1)}, u32[]{:S(2)}, u32[]{:S(2)}) async-start(f32[32,33,128]{2,1,0:T(8,128)} %copy.45), calls=%async_computation | async-start | bytes 1310720 | tf_op jit(solution)/shard_map/all_to_all | solution.py:51
  37.2 36.4 %copy-start.9 = (f32[128]{0:T(128)S(1)}, f32[128]{0:T(128)}, u32[]{:S(2)}) copy-start(f32[128]{0:T(128)} %param.15) | copy-start | bytes 1540
  57.8 15.6 %all-to-all-start.2 = ((f32[32,8,128]{2,1,0:T(8,128)}), f32[32,8,128]{2,1,0:T(8,128)S(1)}, u32[]{:S(2)}, u32[]{:S(2)}) async-start(f32[32,8,128]{2,1,0:T(8,128)} %broadcast_in_dim.34), calls=%async_computation.2 | async-start | bytes 262144 | tf_op jit(solution)/shard_map/all_to_all | solution.py:11

commit v2 on v1

v2 whole, which is shorter than its diff:
```python
import functools

import jax
import jax.numpy as jnp
from jax import lax
from jax.experimental import pallas as pl
from jax.experimental.pallas import tpu as pltpu
from jax.sharding import PartitionSpec as P

HD = 128
PIECES = 4


def log1p_minus(key):
    poly = jnp.float32(1.0 / 7.0)
    for order in range(6, 0, -1):
        poly = poly * key + jnp.float32(1.0 / order)
    return -(key * poly)


def key_of(forget_pre, opening):
    return opening / (1.0 + jnp.exp(forget_pre))


def dense_kernel(
    prompt, forget_weight, value_weight, lower_bound, extra_decay, sent,
    tokens, forget_w, value_w, extra, tot, first_sems, token_sems, extra_sem,
):
    seq_count, span_len, width = tokens.shape
    dests = sent.shape[0]
    row_share = HD // dests
    head_count = forget_w.shape[1] // HD
    groups = head_count * seq_count
    piece = width // PIECES
    first = []
    for p in range(PIECES):
        cut = pl.ds(p * piece, piece)
        first.append((
            pltpu.make_async_copy(prompt.at[0, :, cut], tokens.at[0, :, cut], first_sems.at[p, 0]),
            pltpu.make_async_copy(forget_weight.at[cut], forget_w.at[cut], first_sems.at[p, 1]),
            pltpu.make_async_copy(value_weight.at[cut], value_w.at[cut], first_sems.at[p, 2]),
        ))
    rest = [
        pltpu.make_async_copy(prompt.at[s], tokens.at[s], token_sems.at[s])
        for s in range(1, seq_count)
    ]
    extra_copy = pltpu.make_async_copy(extra_decay, extra, extra_sem)
    for copies in first:
        for copy in copies:
            copy.start()
    extra_copy.start()
    for copy in rest:
        copy.start()

    opening = 1.0 - lower_bound[...]
    row = lax.broadcasted_iota(jnp.int32, (span_len, span_len), 0)
    col = lax.broadcasted_iota(jnp.int32, (span_len, span_len), 1)
    after = jnp.where(col > row, 1.0, 0.0).astype(jnp.bfloat16)

    def finish(s, forget_pre, values):
        key = key_of(forget_pre.astype(jnp.float32), opening)
        log_forget = log1p_minus(key) + extra[s]
        high = log_forget.astype(jnp.bfloat16)
        left = log_forget - high.astype(jnp.float32)
        middle = left.astype(jnp.bfloat16)
        low = (left - middle.astype(jnp.float32)).astype(jnp.bfloat16)
        later = (
            jnp.dot(after, high, preferred_element_type=jnp.float32)
            + jnp.dot(after, middle, preferred_element_type=jnp.float32)
            + jnp.dot(after, low, preferred_element_type=jnp.float32)
        )
        totals = later[:1] + log_forget[:1]
        weighted = (key * jnp.exp(later)).astype(jnp.bfloat16)
        for h in range(head_count):
            cut = slice(h * HD, (h + 1) * HD)
            group = h * seq_count + s
            tot[group : group + 1, :] = totals[:, cut]
            state = lax.dot_general(
                weighted[:, cut], values[:, cut], (((0,), (0,)), ((), ())),
                preferred_element_type=jnp.float32,
            )
            for k in range(dests):
                sent[k, pl.ds(group, row_share, stride=groups), :] = state[
                    k * row_share : (k + 1) * row_share
                ]

    forget_sum = value_sum = None
    for p in range(PIECES):
        for copy in first[p]:
            copy.wait()
        cut = slice(p * piece, (p + 1) * piece)
        part = tokens[0, :, cut]
        forget_part = jnp.dot(part, forget_w[cut], preferred_element_type=jnp.float32)
        value_part = jnp.dot(part, value_w[cut], preferred_element_type=jnp.float32)
        forget_sum = forget_part if p == 0 else forget_sum + forget_part
        value_sum = value_part if p == 0 else value_sum + value_part
    pending = (forget_sum.astype(jnp.bfloat16), value_sum.astype(jnp.bfloat16))
    extra_copy.wait()
    for s in range(1, seq_count):
        rest[s - 1].wait()
        forget_pre = jnp.dot(
            tokens[s], forget_w[...], preferred_element_type=jnp.float32
        ).astype(jnp.bfloat16)
        values = jnp.dot(
            tokens[s], value_w[...], preferred_element_type=jnp.float32
        ).astype(jnp.bfloat16)
        finish(s - 1, *pending)
        pending = (forget_pre, values)
    finish(seq_count - 1, *pending)
    for k in range(dests):
        sent[k, row_share * groups :, :] = tot[...]


def token_kernel(
    pieces, forget_weight, value_weight, lower_bound, new_query, reach, addend, forget_sum, value_sum
):
    step = pl.program_id(0)
    seq_count = pieces.shape[1]
    head_count = forget_weight.shape[1] // HD

    @pl.when(step == 0)
    def _():
        forget_sum[...] = jnp.zeros_like(forget_sum)
        value_sum[...] = jnp.zeros_like(value_sum)

    forget_sum[...] += jnp.dot(pieces[0], forget_weight[...], preferred_element_type=jnp.float32)
    value_sum[...] += jnp.dot(pieces[0], value_weight[...], preferred_element_type=jnp.float32)

    @pl.when(step == pl.num_programs(0) - 1)
    def _():
        def grouped(rows):
            return jnp.concatenate(
                [rows[:, h * HD : (h + 1) * HD] for h in range(head_count)], axis=0
            )

        new_forget = forget_sum[...].astype(jnp.bfloat16).astype(jnp.float32)
        new_value = grouped(value_sum[...].astype(jnp.bfloat16).astype(jnp.float32))
        new_key = key_of(new_forget, 1.0 - lower_bound[...])
        query = new_query[...].astype(jnp.float32)
        query = query / (1.0 + jnp.exp(-query))
        reach[...] = grouped(query * (1.0 - new_key))
        key_sum = jnp.sum(grouped(query * new_key), axis=1, keepdims=True)
        addend[...] = key_sum * new_value


def state_kernel(got, reach, state_cache, shares, *, axis):
    blocks, rows, _ = got.shape
    groups = reach.shape[0]
    row_share = HD // blocks
    head_count, seq_count = state_cache.shape[1:3]
    back = lax.rem(HD - lax.axis_index(axis) * row_share, HD)
    final = [None] * row_share
    later = jnp.zeros((groups, HD), jnp.float32)
    for b in range(blocks - 1, -1, -1):
        scale = pltpu.roll(jnp.exp(later), back, 1)
        for d in range(row_share):
            term = scale[:, d : d + 1] * got[b, d * groups : (d + 1) * groups, :]
            final[d] = term if final[d] is None else final[d] + term
        if b > 0:
            later = later + got[b, row_share * groups :, :]
    own_reach = pltpu.roll(reach[...], back, 1)
    share = None
    for d in range(row_share):
        for h in range(head_count):
            state_cache[d, h] = final[d][h * seq_count : (h + 1) * seq_count].astype(jnp.bfloat16)
        term = own_reach[:, d : d + 1] * final[d]
        share = term if share is None else share + term
    for k in range(blocks):
        shares[k] = share


def read_kernel(shares, addend, read_gain, first_read):
    blocks = shares.shape[0]
    seq_count = first_read.shape[0]
    raw = shares[0]
    for k in range(1, blocks):
        raw = raw + shares[k]
    raw = raw + addend[...]
    mean = jnp.mean(raw * raw, axis=1, keepdims=True)
    normed = raw * lax.rsqrt(mean + 1e-06) * read_gain[...]
    for h in range(first_read.shape[1] // HD):
        first_read[:, h * HD : (h + 1) * HD] = normed[
            h * seq_count : (h + 1) * seq_count
        ].astype(jnp.bfloat16)


def local(
    prompt, forget_weight, value_weight, lower_bound, extra_decay, new_token, new_query, read_gain
):
    seq_count, span_len, width = prompt.shape
    width_dev = forget_weight.shape[1]
    head_count = width_dev // HD
    blocks = lax.axis_size("sp")
    peers = lax.axis_size("tp")
    row_share = HD // blocks
    groups = head_count * seq_count
    rows = (row_share + 1) * groups
    anywhere = pl.BlockSpec(memory_space=pl.ANY)
    vmem = pl.BlockSpec(memory_space=pltpu.VMEM)
    lower_row = lower_bound[None]
    sent = pl.pallas_call(
        dense_kernel,
        out_shape=jax.ShapeDtypeStruct((blocks, rows, HD), jnp.float32),
        in_specs=[anywhere, anywhere, anywhere, vmem, anywhere],
        out_specs=vmem,
        scratch_shapes=[
            pltpu.VMEM((seq_count, span_len, width), jnp.bfloat16),
            pltpu.VMEM((width, width_dev), jnp.bfloat16),
            pltpu.VMEM((width, width_dev), jnp.bfloat16),
            pltpu.VMEM((seq_count, span_len, width_dev), jnp.float32),
            pltpu.VMEM((groups, HD), jnp.float32),
            pltpu.SemaphoreType.DMA((PIECES, 3)),
            pltpu.SemaphoreType.DMA((seq_count,)),
            pltpu.SemaphoreType.DMA,
        ],
        name="dense",
    )(prompt, forget_weight, value_weight, lower_row, extra_decay)
    got = lax.all_to_all(sent, "sp", 0, 0, tiled=True)

    token, _ = lax.optimization_barrier((new_token, sent))
    pieces = lax.all_to_all(
        jnp.broadcast_to(token[None], (peers, *token.shape)), "tp", 0, 0, tiled=True
    )
    part = width // peers
    reach, addend = pl.pallas_call(
        token_kernel,
        grid=(peers,),
        out_shape=[jax.ShapeDtypeStruct((groups, HD), jnp.float32)] * 2,
        in_specs=[
            pl.BlockSpec((1, seq_count, part), lambda i: (i, 0, 0)),
            pl.BlockSpec((part, width_dev), lambda i: (i, 0)),
            pl.BlockSpec((part, width_dev), lambda i: (i, 0)),
            pl.BlockSpec((1, width_dev), lambda i: (0, 0)),
            pl.BlockSpec((seq_count, width_dev), lambda i: (0, 0)),
        ],
        out_specs=[pl.BlockSpec((groups, HD), lambda i: (0, 0))] * 2,
        scratch_shapes=[pltpu.VMEM((seq_count, width_dev), jnp.float32)] * 2,
        name="token",
    )(pieces, forget_weight, value_weight, lower_row, new_query)
    state_cache, shares = pl.pallas_call(
        functools.partial(state_kernel, axis="sp"),
        out_shape=[
            jax.ShapeDtypeStruct((row_share, head_count, seq_count, HD), jnp.bfloat16),
            jax.ShapeDtypeStruct((blocks, groups, HD), jnp.float32),
        ],
        in_specs=[vmem, vmem],
        out_specs=[vmem, vmem],
        name="state",
    )(got, reach)
    shares = lax.all_to_all(shares, "sp", 0, 0, tiled=True)
    first_read = pl.pallas_call(
        read_kernel,
        out_shape=jax.ShapeDtypeStruct((seq_count, width_dev), jnp.bfloat16),
        in_specs=[vmem, vmem, vmem],
        out_specs=vmem,
        name="read",
    )(shares, addend, read_gain[None])
    return (state_cache, first_read)


def solution(mesh):
    return jax.shard_map(
        local,
        mesh=mesh,
        in_specs=(
            P(None, "sp", None),
            P(None, "tp"),
            P(None, "tp"),
            P("tp"),
            P(None, "sp", "tp"),
            P(None, "tp"),
            P(None, "tp"),
            P(),
        ),
        out_specs=(P("sp", "tp", None, None), P(None, "tp")),
        check_vma=False,
    )
```

time: 74.8 us -> 72.7 us (0.972)
  blocking collectives: 0 us -> 25 us
  Pallas kernels: 0 us -> 20.6 us
  matrix products: 12.9 us -> 0 us
  waiting for transfers between devices: 26.9 us -> 14.3 us
  starting transfers between devices: 21.3 us -> 10.9 us
  other arithmetic: 5.74 us -> 0 us
  local copies, waits for them, and re-layouts: 6.48 us -> 0.86 us
    all_to_all x0 -> x2, blocking collectives: none -> 25 us  [the longest x1 15.7 us: local(): shares = lax.all_to_all(shares, 'sp', 0, 0, tiled=True)]
    pallas_call x0 -> x4, Pallas kernels: none -> 20.6 us  [the longest x1 10.3 us: local(): pl.pallas_call(dense_kernel, out_shape=jax.ShapeDtypeStruct((blocks, rows...]
    dot_general x5 -> x0, matrix products: 12.9 us -> none  [the longest x1 4.65 us: local(): jnp.einsum('std,dw->stw', prompt, forget_weight, preferred_element_type=j...]
    all_to_all x3 -> x1, waiting for transfers between devices: 26.9 us -> 14.3 us  [local(): got = lax.all_to_all(sent, 'sp', 0, 0, tiled=True)]
    all_to_all x3 -> x1, starting transfers between devices: 21.3 us -> 10.9 us  [local(): got = lax.all_to_all(sent, 'sp', 0, 0, tiled=True)]
    broadcast_in_dim x2 -> x1, local copies, waits for them, and re-layouts: 2.1 us -> 0.01 us  [local(): jnp.broadcast_to(token[None], (peers, *token.shape))]
    another operation x3 -> x0, other arithmetic: 1.92 us -> none
    sub x1 -> x0, other arithmetic: 1.24 us -> none  [local(): opening = 1.0 - lower_bound]
  transfers between devices with their start and end apart: 3 -> 1, of which waited for: 2 -> 1; matrix products, arithmetic and copies ran while one was open for 28% -> 0% of each run, Pallas kernels for 0% -> 8%
where the time goes in v2:
time: 72.7 us; the launch traced here: 72.3 us
  blocking collectives  25 us (34%)
  Pallas kernels  20.6 us (28%)
  waiting for transfers between devices  14.3 us (20%)
  starting transfers between devices  10.9 us (15%)
  local copies, waits for them, and re-layouts  0.86 us (1%)
    all_to_all x1, blocking collectives, local(): shares = lax.all_to_all(shares, 'sp', 0, 0, tiled=True)  15.7 us
    all_to_all x1, waiting for transfers between devices, local(): got = lax.all_to_all(sent, 'sp', 0, 0, tiled=True)  14.3 us
    all_to_all x1, starting transfers between devices, local(): got = lax.all_to_all(sent, 'sp', 0, 0, tiled=True)  10.9 us
    pallas_call x1, Pallas kernels, local(): pl.pallas_call(dense_kernel, out_shape=jax.ShapeDtypeStruct((blocks, rows...  10.3 us
    all_to_all x1, blocking collectives, local(): lax.all_to_all(jnp.broadcast_to(token[None], (peers, *token.shape)), 'tp'...  9.26 us
    pallas_call x1, Pallas kernels, local(): pl.pallas_call(token_kernel, grid=(peers,), out_shape=[jax.ShapeDtypeStru...  5.9 us
    pallas_call x1, Pallas kernels, local(): pl.pallas_call(functools.partial(state_kernel, axis='sp'), out_shape=[jax...  2.82 us
    pallas_call x1, Pallas kernels, local(): pl.pallas_call(read_kernel, out_shape=jax.ShapeDtypeStruct((seq_count, wi...  1.61 us
  transfers between devices with their start and end apart: 1, of which 1 were waited for; matrix products, arithmetic and copies ran while one was open for 0% of the time, Pallas kernels for 8%

profile of v2, /device:TPU:2, one launch (start us, length us, event | category | flops | bytes accessed | tf_op | source)
XLA Modules:
  0.0 72.3 jit_solution(382710969505470147)
XLA Ops:
  0.6 0.0 copy-start.1
  0.6 10.3 %dense.1 = f32[32,40,128]{2,1,0:T(8,128)} custom-call(bf16[4,192,4096]{2,1,0:T(8,128)(2,1)} %prompt.1, bf16[4096,256]{1,0:T(8,128)(2,1)} %forget_weight.3, bf16[4096,256]{1,0:T(8,128)(2,1)} %value_weight.3, f32[1,256]{1,0:T(1,128)} %bitcast.2, f32[4,192,256]{2,1,0:T(8,128)} %extra_decay.1), custom_call_target="tpu_custom_call" | custom-call | tf_op jit(solution)/shard_map/dense/pallas_call | solution.py:201
  10.9 0.0 copy-done.1
  10.9 9.3 %all_to_all.15.pieces = bf16[8,4,512]{2,1,0:T(4,128)(2,1)} all-to-all(bf16[8,4,512]{2,1,0:T(4,128)(2,1)S(1)} %broadcast_in_dim.13), channel_id=1, replica_groups=mesh['sp'=32,'tp'=8] {'tp'}, dimensions={0} | all-to-all | bytes 65536 | tf_op jit(solution)/shard_map/all_to_all | solution.py:221
  20.2 10.9 %all-to-all-start = ((f32[32,40,128]{2,1,0:T(8,128)}), f32[32,40,128]{2,1,0:T(8,128)S(1)}, u32[]{:S(2)}, u32[]{:S(2)}) async-start(f32[32,40,128]{2,1,0:T(8,128)} %dense.1), calls=%async_computation | async-start | bytes 1310720 | tf_op jit(solution)/shard_map/all_to_all | solution.py:218
  31.1 5.9 %token_.1 = (f32[8,128]{1,0:T(8,128)}, f32[8,128]{1,0:T(8,128)}) custom-call(bf16[8,4,512]{2,1,0:T(4,128)(2,1)} %all_to_all.15.pieces, bf16[4096,256]{1,0:T(8,128)(2,1)} %forget_weight.3, bf16[4096,256]{1,0:T(8,128)(2,1)} %value_weight.3, f32[1,256]{1,0:T(1,128)} %bitcast.3, bf16[4,256]{1,0:T(4,128)(2,1)} %new_query.1), custom_call_target="tpu_custom_call" | custom-call | tf_op jit(solution)/shard_map/token/pallas_call | solution.py:225
  37.0 14.3 %all-to-all-done.got = f32[32,40,128]{2,1,0:T(8,128)S(1)} async-done(((f32[32,40,128]{2,1,0:T(8,128)}), f32[32,40,128]{2,1,0:T(8,128)S(1)}, u32[]{:S(2)}, u32[]{:S(2)}) %all-to-all-start) | async-done | bytes 655392 | tf_op jit(solution)/shard_map/all_to_all | solution.py:218
  51.3 0.0 copy-start
  51.3 0.8 %copy-done = f32[32,40,128]{2,1,0:T(8,128)} copy-done((f32[32,40,128]{2,1,0:T(8,128)}, f32[32,40,128]{2,1,0:T(8,128)S(1)}, u32[]{:S(2)}) %copy-start) | copy-done | bytes 655384
  52.2 2.8 %state.1 = (bf16[4,2,4,128]{3,2,1,0:T(4,128)(2,1)}, f32[32,8,128]{2,1,0:T(8,128)}) custom-call(f32[32,40,128]{2,1,0:T(8,128)} %copy-done, f32[8,128]{1,0:T(8,128)} %get-tuple-element.8.reach), custom_call_target="tpu_custom_call" | custom-call | tf_op jit(solution)/shard_map/state/pallas_call | solution.py:240
  55.0 15.7 %all_to_all.16.shares = f32[32,8,128]{2,1,0:T(8,128)} all-to-all(f32[32,8,128]{2,1,0:T(8,128)} %get-tuple-element.10), channel_id=1, replica_groups=mesh['sp'=32,'tp'=8] {'sp'}, dimensions={0} | all-to-all | bytes 262144 | tf_op jit(solution)/shard_map/all_to_all | solution.py:250
  70.7 1.6 %read.1 = bf16[4,256]{1,0:T(4,128)(2,1)} custom-call(f32[32,8,128]{2,1,0:T(8,128)} %all_to_all.16.shares, f32[8,128]{1,0:T(8,128)} %get-tuple-element.11.addend, f32[1,128]{1,0:T(1,128)} %bitcast.4), custom_call_target="tpu_custom_call" | custom-call | tf_op jit(solution)/shard_map/read/pallas_call | solution.py:251
  (1 shorter events, 0.0 us)
Async XLA Ops:
  0.6 10.3 %copy-start.1 = (bf16[4,512]{1,0:T(4,128)(2,1)S(1)}, bf16[4,512]{1,0:T(4,128)(2,1)}, u32[]{:S(2)}) copy-start(bf16[4,512]{1,0:T(4,128)(2,1)} %param.13) | copy-start | bytes 12292
  20.2 31.1 %all-to-all-start = ((f32[32,40,128]{2,1,0:T(8,128)}), f32[32,40,128]{2,1,0:T(8,128)S(1)}, u32[]{:S(2)}, u32[]{:S(2)}) async-start(f32[32,40,128]{2,1,0:T(8,128)} %dense.1), calls=%async_computation | async-start | bytes 1310720 | tf_op jit(solution)/shard_map/all_to_all | solution.py:218
  51.3 0.8 %copy-start = (f32[32,40,128]{2,1,0:T(8,128)}, f32[32,40,128]{2,1,0:T(8,128)S(1)}, u32[]{:S(2)}) copy-start(f32[32,40,128]{2,1,0:T(8,128)S(1)} %all-to-all-done.got) | copy-start | bytes 1966084

commit v3 on v2

--- a/solution.py
+++ b/solution.py
@@ -24,7 +24,7 @@
 
 def dense_kernel(
     prompt, forget_weight, value_weight, lower_bound, extra_decay, sent,
-    tokens, forget_w, value_w, extra, tot, first_sems, token_sems, extra_sem,
+    tokens, forget_w, value_w, extra, lower, tot, first_sems, token_sems, extra_sem, lower_sem,
 ):
     seq_count, span_len, width = tokens.shape
     dests = sent.shape[0]
@@ -45,6 +45,8 @@
         for s in range(1, seq_count)
     ]
     extra_copy = pltpu.make_async_copy(extra_decay, extra, extra_sem)
+    lower_copy = pltpu.make_async_copy(lower_bound, lower, lower_sem)
+    lower_copy.start()
     for copies in first:
         for copy in copies:
             copy.start()
@@ -52,7 +54,6 @@
     for copy in rest:
         copy.start()
 
-    opening = 1.0 - lower_bound[...]
     row = lax.broadcasted_iota(jnp.int32, (span_len, span_len), 0)
     col = lax.broadcasted_iota(jnp.int32, (span_len, span_len), 1)
     after = jnp.where(col > row, 1.0, 0.0).astype(jnp.bfloat16)
@@ -96,6 +97,8 @@
         value_sum = value_part if p == 0 else value_sum + value_part
     pending = (forget_sum.astype(jnp.bfloat16), value_sum.astype(jnp.bfloat16))
     extra_copy.wait()
+    lower_copy.wait()
+    opening = 1.0 - lower[...]
     for s in range(1, seq_count):
         rest[s - 1].wait()
         forget_pre = jnp.dot(
@@ -112,39 +115,46 @@
 
 
 def token_kernel(
-    pieces, forget_weight, value_weight, lower_bound, new_query, reach, addend, forget_sum, value_sum
+    own, pair, far, forget_weight, value_weight, lower_bound, new_query, reach, addend,
+    forget_w, value_w, whole, sems, *, axis
 ):
-    step = pl.program_id(0)
-    seq_count = pieces.shape[1]
-    head_count = forget_weight.shape[1] // HD
-
-    @pl.when(step == 0)
-    def _():
-        forget_sum[...] = jnp.zeros_like(forget_sum)
-        value_sum[...] = jnp.zeros_like(value_sum)
-
-    forget_sum[...] += jnp.dot(pieces[0], forget_weight[...], preferred_element_type=jnp.float32)
-    value_sum[...] += jnp.dot(pieces[0], value_weight[...], preferred_element_type=jnp.float32)
-
-    @pl.when(step == pl.num_programs(0) - 1)
-    def _():
-        def grouped(rows):
-            return jnp.concatenate(
-                [rows[:, h * HD : (h + 1) * HD] for h in range(head_count)], axis=0
-            )
-
-        new_forget = forget_sum[...].astype(jnp.bfloat16).astype(jnp.float32)
-        new_value = grouped(value_sum[...].astype(jnp.bfloat16).astype(jnp.float32))
-        new_key = key_of(new_forget, 1.0 - lower_bound[...])
-        query = new_query[...].astype(jnp.float32)
-        query = query / (1.0 + jnp.exp(-query))
-        reach[...] = grouped(query * (1.0 - new_key))
-        key_sum = jnp.sum(grouped(query * new_key), axis=1, keepdims=True)
-        addend[...] = key_sum * new_value
+    copies = [
+        pltpu.make_async_copy(forget_weight, forget_w, sems.at[0]),
+        pltpu.make_async_copy(value_weight, value_w, sems.at[1]),
+    ]
+    for copy in copies:
+        copy.start()
+    _, part = own.shape
+    peers = whole.shape[1] // part
+    head_count = forget_w.shape[1] // HD
+    me = lax.axis_index(axis)
+    held = [(me, own[...]), (me ^ 1, pair[...])]
+    for step in range(1, peers // 2):
+        source = lax.rem(me + peers - 2 * step, peers)
+        held += [(source, far[step - 1, 0]), (source ^ 1, far[step - 1, 1])]
+    for source, rows in held:
+        whole[:, pl.ds(pl.multiple_of(source * part, part), part)] = rows.astype(jnp.float32)
+    token = whole[...].astype(jnp.bfloat16)
+    for copy in copies:
+        copy.wait()
+
+    def grouped(rows):
+        return jnp.concatenate([rows[:, h * HD : (h + 1) * HD] for h in range(head_count)], axis=0)
+
+    def rounded(weight):
+        out = jnp.dot(token, weight[...], preferred_element_type=jnp.float32)
+        return out.astype(jnp.bfloat16).astype(jnp.float32)
+
+    new_key = key_of(rounded(forget_w), 1.0 - lower_bound[...])
+    query = new_query[...].astype(jnp.float32)
+    query = query / (1.0 + jnp.exp(-query))
+    reach[...] = grouped(query * (1.0 - new_key))
+    key_sum = jnp.sum(grouped(query * new_key), axis=1, keepdims=True)
+    addend[...] = key_sum * grouped(rounded(value_w))
 
 
 def state_kernel(got, reach, state_cache, shares, *, axis):
-    blocks, rows, _ = got.shape
+    blocks, _, _ = got.shape
     groups = reach.shape[0]
     row_share = HD // blocks
     head_count, seq_count = state_cache.shape[1:3]
@@ -195,59 +205,60 @@
     row_share = HD // blocks
     groups = head_count * seq_count
     rows = (row_share + 1) * groups
-    anywhere = pl.BlockSpec(memory_space=pl.ANY)
+    anywhere = pl.BlockSpec(memory_space=pltpu.HBM)
     vmem = pl.BlockSpec(memory_space=pltpu.VMEM)
     lower_row = lower_bound[None]
     sent = pl.pallas_call(
         dense_kernel,
         out_shape=jax.ShapeDtypeStruct((blocks, rows, HD), jnp.float32),
-        in_specs=[anywhere, anywhere, anywhere, vmem, anywhere],
+        in_specs=[anywhere] * 5,
         out_specs=vmem,
         scratch_shapes=[
             pltpu.VMEM((seq_count, span_len, width), jnp.bfloat16),
             pltpu.VMEM((width, width_dev), jnp.bfloat16),
             pltpu.VMEM((width, width_dev), jnp.bfloat16),
             pltpu.VMEM((seq_count, span_len, width_dev), jnp.float32),
+            pltpu.VMEM((1, width_dev), jnp.float32),
             pltpu.VMEM((groups, HD), jnp.float32),
             pltpu.SemaphoreType.DMA((PIECES, 3)),
             pltpu.SemaphoreType.DMA((seq_count,)),
+            pltpu.SemaphoreType.DMA,
             pltpu.SemaphoreType.DMA,
         ],
         name="dense",
     )(prompt, forget_weight, value_weight, lower_row, extra_decay)
     got = lax.all_to_all(sent, "sp", 0, 0, tiled=True)
-
     token, _ = lax.optimization_barrier((new_token, sent))
-    pieces = lax.all_to_all(
-        jnp.broadcast_to(token[None], (peers, *token.shape)), "tp", 0, 0, tiled=True
-    )
-    part = width // peers
+    pair = lax.ppermute(token, "tp", [(i, i ^ 1) for i in range(peers)])
+    both = jnp.stack([token, pair])
+    far = []
+    for step in range(1, peers // 2):
+        far.append(lax.ppermute(both, "tp", [(i, (i + 2 * step) % peers) for i in range(peers)]))
     reach, addend = pl.pallas_call(
-        token_kernel,
-        grid=(peers,),
+        functools.partial(token_kernel, axis="tp"),
         out_shape=[jax.ShapeDtypeStruct((groups, HD), jnp.float32)] * 2,
-        in_specs=[
-            pl.BlockSpec((1, seq_count, part), lambda i: (i, 0, 0)),
-            pl.BlockSpec((part, width_dev), lambda i: (i, 0)),
-            pl.BlockSpec((part, width_dev), lambda i: (i, 0)),
-            pl.BlockSpec((1, width_dev), lambda i: (0, 0)),
-            pl.BlockSpec((seq_count, width_dev), lambda i: (0, 0)),
+        in_specs=[vmem, vmem, vmem, anywhere, anywhere, vmem, vmem],
+        out_specs=[vmem] * 2,
+        scratch_shapes=[
+            pltpu.VMEM((width, width_dev), jnp.bfloat16),
+            pltpu.VMEM((width, width_dev), jnp.bfloat16),
+            pltpu.VMEM((seq_count, width), jnp.float32),
+            pltpu.SemaphoreType.DMA((2,)),
         ],
-        out_specs=[pl.BlockSpec((groups, HD), lambda i: (0, 0))] * 2,
-        scratch_shapes=[pltpu.VMEM((seq_count, width_dev), jnp.float32)] * 2,
         name="token",
-    )(pieces, forget_weight, value_weight, lower_row, new_query)
+    )(token, pair, jnp.stack(far), forget_weight, value_weight, lower_row, new_query)
+    got = pltpu.with_memory_space_constraint(got, pltpu.VMEM)
     state_cache, shares = pl.pallas_call(
         functools.partial(state_kernel, axis="sp"),
         out_shape=[
             jax.ShapeDtypeStruct((row_share, head_count, seq_count, HD), jnp.bfloat16),
-            jax.ShapeDtypeStruct((blocks, groups, HD), jnp.float32),
+            pltpu.VMEM((blocks, groups, HD), jnp.float32),
         ],
         in_specs=[vmem, vmem],
         out_specs=[vmem, vmem],
         name="state",
     )(got, reach)
-    shares = lax.all_to_all(shares, "sp", 0, 0, tiled=True)
+    shares = pltpu.with_memory_space_constraint(lax.all_to_all(shares, "sp", 0, 0, tiled=True), pltpu.VMEM)
     first_read = pl.pallas_call(
         read_kernel,
         out_shape=jax.ShapeDtypeStruct((seq_count, width_dev), jnp.bfloat16),

time: 72.7 us -> 61.4 us (0.84)
  blocking collectives: 25 us -> 15.4 us
  starting transfers between devices: 10.9 us -> 16.4 us
  waiting for transfers between devices: 14.3 us -> 10.3 us
  Pallas kernels: 20.6 us -> 17.7 us
  local copies, waits for them, and re-layouts: 0.86 us -> 0.01 us
    all_to_all x2 -> x1, blocking collectives: 25 us -> 15.4 us  [local(): lax.all_to_all(shares, 'sp', 0, 0, tiled=True)]
    all_to_all x1, waiting for transfers between devices: 14.3 us -> 7.26 us  [local(): got = lax.all_to_all(sent, 'sp', 0, 0, tiled=True)]
    ppermute x0 -> x4, starting transfers between devices: none -> 4.93 us  [the longest x3 4.84 us: local(): lax.ppermute(both, 'tp', [(i, (i + 2 * step) % peers) for i in range(peer...]
    ppermute x0 -> x4, waiting for transfers between devices: none -> 3 us  [the longest x3 1.84 us: local(): lax.ppermute(both, 'tp', [(i, (i + 2 * step) % peers) for i in range(peer...]
    pallas_call x1, Pallas kernels: 5.9 us -> 4.37 us  [local(): pl.pallas_call(functools.partial(token_kernel, axis='tp'), out_shape=[jax...]
    unnamed x4, local copies, waits for them, and re-layouts: 0.85 us -> 0.01 us
  transfers between devices with their start and end apart: 1 -> 5, of which waited for: 1 -> 4; matrix products, arithmetic and copies ran while one was open for 0% -> 1% of each run, Pallas kernels for 8% -> 7%
where the time goes in v3:
time: 61.4 us; the launch traced here: 61.1 us
  Pallas kernels  17.7 us (29%)
  starting transfers between devices  16.4 us (27%)
  blocking collectives  15.4 us (25%)
  waiting for transfers between devices  10.3 us (17%)
  between operations  0.69 us (1%)
  other arithmetic  0.63 us (1%)
    all_to_all x1, blocking collectives, local(): lax.all_to_all(shares, 'sp', 0, 0, tiled=True)  15.4 us
    all_to_all x1, starting transfers between devices, local(): got = lax.all_to_all(sent, 'sp', 0, 0, tiled=True)  11.5 us
    pallas_call x1, Pallas kernels, local(): pl.pallas_call(dense_kernel, out_shape=jax.ShapeDtypeStruct((blocks, rows...  9.58 us
    all_to_all x1, waiting for transfers between devices, local(): got = lax.all_to_all(sent, 'sp', 0, 0, tiled=True)  7.26 us
    ppermute x3, starting transfers between devices, local(): lax.ppermute(both, 'tp', [(i, (i + 2 * step) % peers) for i in range(peer...  4.84 us
    pallas_call x1, Pallas kernels, local(): pl.pallas_call(functools.partial(token_kernel, axis='tp'), out_shape=[jax...  4.37 us
    pallas_call x1, Pallas kernels, local(): pl.pallas_call(functools.partial(state_kernel, axis='sp'), out_shape=[jax...  2.35 us
    ppermute x3, waiting for transfers between devices, local(): lax.ppermute(both, 'tp', [(i, (i + 2 * step) % peers) for i in range(peer...  1.84 us
  transfers between devices with their start and end apart: 5, of which 4 were waited for; matrix products, arithmetic and copies ran while one was open for 1% of the time, Pallas kernels for 7%

profile of v3, /device:TPU:2, one launch (start us, length us, event | category | flops | bytes accessed | tf_op | source)
XLA Modules:
  0.0 61.1 jit_solution(5517484306040815463)
XLA Ops:
  0.6 0.0 copy-start
  0.6 9.6 %dense.1 = f32[32,40,128]{2,1,0:T(8,128)} custom-call(bf16[4,192,4096]{2,1,0:T(8,128)(2,1)} %prompt.1, bf16[4096,256]{1,0:T(8,128)(2,1)} %forget_weight.3, bf16[4096,256]{1,0:T(8,128)(2,1)} %value_weight.3, f32[1,256]{1,0:T(1,128)} %bitcast.12, f32[4,192,256]{2,1,0:T(8,128)} %extra_decay.1), custom_call_target="tpu_custom_call" | custom-call | tf_op jit(solution)/shard_map/dense/pallas_call | solution.py:211
  10.2 11.5 %all-to-all-start = ((f32[32,40,128]{2,1,0:T(8,128)}), f32[32,40,128]{2,1,0:T(8,128)S(1)}, u32[]{:S(2)}, u32[]{:S(2)}) async-start(f32[32,40,128]{2,1,0:T(8,128)} %dense.1), calls=%async_computation | async-start | bytes 1310720 | tf_op jit(solution)/shard_map/all_to_all | solution.py:230
  21.7 0.0 copy-done
  21.7 0.1 collective-permute-start
  21.8 1.2 %collective-permute-done.pair = bf16[4,512]{1,0:T(4,128)(2,1)S(1)} collective-permute-done((bf16[4,512]{1,0:T(4,128)(2,1)S(1)}, bf16[4,512]{1,0:T(4,128)(2,1)S(1)}, u32[]{:S(2)}, u32[]{:S(2)}) %collective-permute-start) | collective-permute-done | bytes 4128 | tf_op jit(solution)/shard_map/ppermute | solution.py:232
  23.0 0.0 copy-start.1
  23.0 0.6 %collective-permute-start.3 = (bf16[2,4,512]{2,1,0:T(4,128)(2,1)S(1)}, bf16[2,4,512]{2,1,0:T(4,128)(2,1)S(1)}, u32[]{:S(2)}, u32[]{:S(2)}) collective-permute-start(bf16[2,4,512]{2,1,0:T(4,128)(2,1)S(1)} %pad_maximum_fusion.1), channel_id=1, source_target_pairs={{0,6},{1,7},{2,0},{3,1},{4,2},{5,3},{6,4},{7,5},{8,14},{9,15},{10,... | collective-permute-start | bytes 24584 | tf_op jit(solution)/shard_map/ppermute | solution.py:236
  23.6 2.4 %collective-permute-start.2 = (bf16[2,4,512]{2,1,0:T(4,128)(2,1)S(1)}, bf16[2,4,512]{2,1,0:T(4,128)(2,1)S(1)}, u32[]{:S(2)}, u32[]{:S(2)}) collective-permute-start(bf16[2,4,512]{2,1,0:T(4,128)(2,1)S(1)} %pad_maximum_fusion.1), channel_id=1, source_target_pairs={{0,4},{1,5},{2,6},{3,7},{4,0},{5,1},{6,2},{7,3},{8,12},{9,13},{10,... | collective-permute-start | bytes 24584 | tf_op jit(solution)/shard_map/ppermute | solution.py:236
  26.0 1.8 %collective-permute-start.1 = (bf16[2,4,512]{2,1,0:T(4,128)(2,1)S(1)}, bf16[2,4,512]{2,1,0:T(4,128)(2,1)S(1)}, u32[]{:S(2)}, u32[]{:S(2)}) collective-permute-start(bf16[2,4,512]{2,1,0:T(4,128)(2,1)S(1)} %pad_maximum_fusion.1), channel_id=1, source_target_pairs={{0,2},{1,3},{2,4},{3,5},{4,6},{5,7},{6,0},{7,1},{8,10},{9,11},{10,... | collective-permute-start | bytes 24584 | tf_op jit(solution)/shard_map/ppermute | solution.py:236
  27.8 0.0 collective-permute-done.3
  27.9 0.9 %collective-permute-done.2 = bf16[2,4,512]{2,1,0:T(4,128)(2,1)S(1)} collective-permute-done((bf16[2,4,512]{2,1,0:T(4,128)(2,1)S(1)}, bf16[2,4,512]{2,1,0:T(4,128)(2,1)S(1)}, u32[]{:S(2)}, u32[]{:S(2)}) %collective-permute-start.2) | collective-permute-done | bytes 8224 | tf_op jit(solution)/shard_map/ppermute | solution.py:236
  28.8 0.9 %collective-permute-done.1 = bf16[2,4,512]{2,1,0:T(4,128)(2,1)S(1)} collective-permute-done((bf16[2,4,512]{2,1,0:T(4,128)(2,1)S(1)}, bf16[2,4,512]{2,1,0:T(4,128)(2,1)S(1)}, u32[]{:S(2)}, u32[]{:S(2)}) %collective-permute-start.1) | collective-permute-done | bytes 8224 | tf_op jit(solution)/shard_map/ppermute | solution.py:236
  29.7 0.6 %pad_maximum_fusion.far = bf16[3,2,4,512]{3,2,1,0:T(4,128)(2,1)} fusion(bf16[1,2,4,512]{3,2,1,0:T(4,128)(2,1)S(1)} %bitcast.9, bf16[1,2,4,512]{3,2,1,0:T(4,128)(2,1)S(1)} %bitcast.10, bf16[1,2,4,512]{3,2,1,0:T(4,128)(2,1)S(1)} %bitcast.11), kind=kLoop, calls=%fused_computation | loop fusion | flops 24576 | bytes 49152 | tf_op jit(solution)/shard_map/stack | solution.py:249
  30.3 0.0 copy-done.1
  30.3 4.4 %token_.1 = (f32[8,128]{1,0:T(8,128)}, f32[8,128]{1,0:T(8,128)}) custom-call(bf16[4,512]{1,0:T(4,128)(2,1)} %own, bf16[4,512]{1,0:T(4,128)(2,1)} %copy-done.1, bf16[3,2,4,512]{3,2,1,0:T(4,128)(2,1)} %pad_maximum_fusion.far, bf16[4096,256]{1,0:T(8,128)(2,1)} %forget_weight.3, bf16[4096,256]{1,0:T(8,128)(2,1)} %value_weight.3, f32[1,256]{1,0:T(1,128)} %bitcast.13, ...), custom_call_target="tpu_custom_call" | custom-call | tf_op jit(solution)/shard_map/token/pallas_call | solution.py:237
  34.7 7.3 %all-to-all-done.got = f32[32,40,128]{2,1,0:T(8,128)S(1)} async-done(((f32[32,40,128]{2,1,0:T(8,128)}), f32[32,40,128]{2,1,0:T(8,128)S(1)}, u32[]{:S(2)}, u32[]{:S(2)}) %all-to-all-start) | async-done | bytes 655392 | tf_op jit(solution)/shard_map/all_to_all | solution.py:230
  42.0 2.3 %state.1 = (bf16[4,2,4,128]{3,2,1,0:T(4,128)(2,1)}, f32[32,8,128]{2,1,0:T(8,128)S(1)}) custom-call(f32[32,40,128]{2,1,0:T(8,128)S(1)} %all-to-all-done.got, f32[8,128]{1,0:T(8,128)} %get-tuple-element.8.reach), custom_call_target="tpu_custom_call" | custom-call | tf_op jit(solution)/shard_map/state/pallas_call | solution.py:251
  44.3 15.4 %all_to_all.10.shares = f32[32,8,128]{2,1,0:T(8,128)S(1)} all-to-all(f32[32,8,128]{2,1,0:T(8,128)S(1)} %get-tuple-element.10), channel_id=1, replica_groups=mesh['sp'=32,'tp'=8] {'sp'}, dimensions={0} | all-to-all | bytes 262144 | tf_op jit(solution)/shard_map/all_to_all | solution.py:261
  59.7 1.4 %read.1 = bf16[4,256]{1,0:T(4,128)(2,1)} custom-call(f32[32,8,128]{2,1,0:T(8,128)S(1)} %all_to_all.10.shares, f32[8,128]{1,0:T(8,128)} %get-tuple-element.11.addend, f32[1,128]{1,0:T(1,128)} %bitcast.14), custom_call_target="tpu_custom_call" | custom-call | tf_op jit(solution)/shard_map/read/pallas_call | solution.py:262
  (1 shorter events, 0.0 us)
Async XLA Ops:
  0.6 21.1 %copy-start = (bf16[4,512]{1,0:T(4,128)(2,1)S(1)}, bf16[4,512]{1,0:T(4,128)(2,1)}, u32[]{:S(2)}) copy-start(bf16[4,512]{1,0:T(4,128)(2,1)} %own) | copy-start | bytes 12292
  10.2 31.7 %all-to-all-start = ((f32[32,40,128]{2,1,0:T(8,128)}), f32[32,40,128]{2,1,0:T(8,128)S(1)}, u32[]{:S(2)}, u32[]{:S(2)}) async-start(f32[32,40,128]{2,1,0:T(8,128)} %dense.1), calls=%async_computation | async-start | bytes 1310720 | tf_op jit(solution)/shard_map/all_to_all | solution.py:230
  21.7 1.3 %collective-permute-start = (bf16[4,512]{1,0:T(4,128)(2,1)S(1)}, bf16[4,512]{1,0:T(4,128)(2,1)S(1)}, u32[]{:S(2)}, u32[]{:S(2)}) collective-permute-start(bf16[4,512]{1,0:T(4,128)(2,1)S(1)} %copy-done), channel_id=1, source_target_pairs={{0,1},{1,0},{2,3},{3,2},{4,5},{5,4},{6,7},{7,6},{8,9},{9,8},{10,11... | collective-permute-start | bytes 12296 | tf_op jit(solution)/shard_map/ppermute | solution.py:232
  23.0 7.3 %copy-start.1 = (bf16[4,512]{1,0:T(4,128)(2,1)}, bf16[4,512]{1,0:T(4,128)(2,1)S(1)}, u32[]{:S(2)}) copy-start(bf16[4,512]{1,0:T(4,128)(2,1)S(1)} %collective-permute-done.pair) | copy-start | bytes 12292
  23.0 4.8 %collective-permute-start.3 = (bf16[2,4,512]{2,1,0:T(4,128)(2,1)S(1)}, bf16[2,4,512]{2,1,0:T(4,128)(2,1)S(1)}, u32[]{:S(2)}, u32[]{:S(2)}) collective-permute-start(bf16[2,4,512]{2,1,0:T(4,128)(2,1)S(1)} %pad_maximum_fusion.1), channel_id=1, source_target_pairs={{0,6},{1,7},{2,0},{3,1},{4,2},{5,3},{6,4},{7,5},{8,14},{9,15},{10,... | collective-permute-start | bytes 24584 | tf_op jit(solution)/shard_map/ppermute | solution.py:236
  23.6 5.2 %collective-permute-start.2 = (bf16[2,4,512]{2,1,0:T(4,128)(2,1)S(1)}, bf16[2,4,512]{2,1,0:T(4,128)(2,1)S(1)}, u32[]{:S(2)}, u32[]{:S(2)}) collective-permute-start(bf16[2,4,512]{2,1,0:T(4,128)(2,1)S(1)} %pad_maximum_fusion.1), channel_id=1, source_target_pairs={{0,4},{1,5},{2,6},{3,7},{4,0},{5,1},{6,2},{7,3},{8,12},{9,13},{10,... | collective-permute-start | bytes 24584 | tf_op jit(solution)/shard_map/ppermute | solution.py:236
  26.0 3.7 %collective-permute-start.1 = (bf16[2,4,512]{2,1,0:T(4,128)(2,1)S(1)}, bf16[2,4,512]{2,1,0:T(4,128)(2,1)S(1)}, u32[]{:S(2)}, u32[]{:S(2)}) collective-permute-start(bf16[2,4,512]{2,1,0:T(4,128)(2,1)S(1)} %pad_maximum_fusion.1), channel_id=1, source_target_pairs={{0,2},{1,3},{2,4},{3,5},{4,6},{5,7},{6,0},{7,1},{8,10},{9,11},{10,... | collective-permute-start | bytes 24584 | tf_op jit(solution)/shard_map/ppermute | solution.py:236

commit v4 on v3

--- a/solution.py
+++ b/solution.py
@@ -9,6 +9,7 @@
 
 HD = 128
 PIECES = 4
+AHEAD = 5
 
 
 def log1p_minus(key):
@@ -24,7 +25,7 @@
 
 def dense_kernel(
     prompt, forget_weight, value_weight, lower_bound, extra_decay, sent,
-    tokens, forget_w, value_w, extra, lower, tot, first_sems, token_sems, extra_sem, lower_sem,
+    tokens, forget_w, value_w, extra, lower, tot, sems,
 ):
     seq_count, span_len, width = tokens.shape
     dests = sent.shape[0]
@@ -32,33 +33,49 @@
     head_count = forget_w.shape[1] // HD
     groups = head_count * seq_count
     piece = width // PIECES
-    first = []
+    groups_in = []
+
+    def group(*pairs):
+        base = sum(len(copies) for copies in groups_in)
+        groups_in.append([
+            pltpu.make_async_copy(source, target, sems.at[base + i])
+            for i, (source, target) in enumerate(pairs)
+        ])
+
     for p in range(PIECES):
         cut = pl.ds(p * piece, piece)
-        first.append((
-            pltpu.make_async_copy(prompt.at[0, :, cut], tokens.at[0, :, cut], first_sems.at[p, 0]),
-            pltpu.make_async_copy(forget_weight.at[cut], forget_w.at[cut], first_sems.at[p, 1]),
-            pltpu.make_async_copy(value_weight.at[cut], value_w.at[cut], first_sems.at[p, 2]),
-        ))
-    rest = [
-        pltpu.make_async_copy(prompt.at[s], tokens.at[s], token_sems.at[s])
-        for s in range(1, seq_count)
-    ]
-    extra_copy = pltpu.make_async_copy(extra_decay, extra, extra_sem)
-    lower_copy = pltpu.make_async_copy(lower_bound, lower, lower_sem)
-    lower_copy.start()
-    for copies in first:
-        for copy in copies:
-            copy.start()
-    extra_copy.start()
-    for copy in rest:
-        copy.start()
+        group(
+            (prompt.at[0, :, cut], tokens.at[0, :, cut]),
+            (forget_weight.at[cut], forget_w.at[cut]),
+            (value_weight.at[cut], value_w.at[cut]),
+        )
+    half = span_len // 2
+    for s in range(1, seq_count):
+        pairs = [
+            (prompt.at[s, pl.ds(at, half)], tokens.at[s, pl.ds(at, half)]) for at in (0, half)
+        ]
+        if s == 1:
+            pairs += [(extra_decay, extra), (lower_bound, lower)]
+        group(*pairs)
+
+    def start(at):
+        if at < len(groups_in):
+            for copy in groups_in[at]:
+                copy.start()
+
+    def arrive(at):
+        for copy in groups_in[at]:
+            copy.wait()
+        start(at + AHEAD)
+
+    for at in range(AHEAD):
+        start(at)
 
     row = lax.broadcasted_iota(jnp.int32, (span_len, span_len), 0)
     col = lax.broadcasted_iota(jnp.int32, (span_len, span_len), 1)
     after = jnp.where(col > row, 1.0, 0.0).astype(jnp.bfloat16)
 
-    def finish(s, forget_pre, values):
+    def finish(s, opening, forget_pre, values):
         key = key_of(forget_pre.astype(jnp.float32), opening)
         log_forget = log1p_minus(key) + extra[s]
         high = log_forget.astype(jnp.bfloat16)
@@ -87,8 +104,7 @@
 
     forget_sum = value_sum = None
     for p in range(PIECES):
-        for copy in first[p]:
-            copy.wait()
+        arrive(p)
         cut = slice(p * piece, (p + 1) * piece)
         part = tokens[0, :, cut]
         forget_part = jnp.dot(part, forget_w[cut], preferred_element_type=jnp.float32)
@@ -96,28 +112,29 @@
         forget_sum = forget_part if p == 0 else forget_sum + forget_part
         value_sum = value_part if p == 0 else value_sum + value_part
     pending = (forget_sum.astype(jnp.bfloat16), value_sum.astype(jnp.bfloat16))
-    extra_copy.wait()
-    lower_copy.wait()
-    opening = 1.0 - lower[...]
+    opening = None
     for s in range(1, seq_count):
-        rest[s - 1].wait()
+        arrive(PIECES + s - 1)
+        opening = 1.0 - lower[...]
         forget_pre = jnp.dot(
             tokens[s], forget_w[...], preferred_element_type=jnp.float32
         ).astype(jnp.bfloat16)
         values = jnp.dot(
             tokens[s], value_w[...], preferred_element_type=jnp.float32
         ).astype(jnp.bfloat16)
-        finish(s - 1, *pending)
+        finish(s - 1, opening, *pending)
         pending = (forget_pre, values)
-    finish(seq_count - 1, *pending)
+    finish(seq_count - 1, opening, *pending)
     for k in range(dests):
         sent[k, row_share * groups :, :] = tot[...]
 
 
 def token_kernel(
-    own, pair, far, forget_weight, value_weight, lower_bound, new_query, reach, addend,
-    forget_w, value_w, whole, sems, *, axis
+    own, pair, *refs, axis
 ):
+    far = refs[:-10]
+    forget_weight, value_weight, lower_bound, new_query, reach, addend = refs[-10:-4]
+    forget_w, value_w, whole, sems = refs[-4:]
     copies = [
         pltpu.make_async_copy(forget_weight, forget_w, sems.at[0]),
         pltpu.make_async_copy(value_weight, value_w, sems.at[1]),
@@ -131,7 +148,7 @@
     held = [(me, own[...]), (me ^ 1, pair[...])]
     for step in range(1, peers // 2):
         source = lax.rem(me + peers - 2 * step, peers)
-        held += [(source, far[step - 1, 0]), (source ^ 1, far[step - 1, 1])]
+        held += [(source, far[step - 1][0]), (source ^ 1, far[step - 1][1])]
     for source, rows in held:
         whole[:, pl.ds(pl.multiple_of(source * part, part), part)] = rows.astype(jnp.float32)
     token = whole[...].astype(jnp.bfloat16)
@@ -179,7 +196,8 @@
         shares[k] = share
 
 
-def read_kernel(shares, addend, read_gain, first_read):
+def read_kernel(shares, addend, read_gain, final, state_cache, first_read):
+    state_cache[...] = final[...]
     blocks = shares.shape[0]
     seq_count = first_read.shape[0]
     raw = shares[0]
@@ -192,6 +210,10 @@
         first_read[:, h * HD : (h + 1) * HD] = normed[
             h * seq_count : (h + 1) * seq_count
         ].astype(jnp.bfloat16)
+
+
+def near(array):
+    return pltpu.with_memory_space_constraint(array, pltpu.VMEM)
 
 
 def local(
@@ -220,10 +242,7 @@
             pltpu.VMEM((seq_count, span_len, width_dev), jnp.float32),
             pltpu.VMEM((1, width_dev), jnp.float32),
             pltpu.VMEM((groups, HD), jnp.float32),
-            pltpu.SemaphoreType.DMA((PIECES, 3)),
-            pltpu.SemaphoreType.DMA((seq_count,)),
-            pltpu.SemaphoreType.DMA,
-            pltpu.SemaphoreType.DMA,
+            pltpu.SemaphoreType.DMA((3 * PIECES + 2 * (seq_count - 1) + 2,)),
         ],
         name="dense",
     )(prompt, forget_weight, value_weight, lower_row, extra_decay)
@@ -233,11 +252,13 @@
     both = jnp.stack([token, pair])
     far = []
     for step in range(1, peers // 2):
-        far.append(lax.ppermute(both, "tp", [(i, (i + 2 * step) % peers) for i in range(peers)]))
+        far.append(
+            lax.ppermute(both, "tp", [(i, (i + 2 * step) % peers) for i in range(peers)])
+        )
     reach, addend = pl.pallas_call(
         functools.partial(token_kernel, axis="tp"),
-        out_shape=[jax.ShapeDtypeStruct((groups, HD), jnp.float32)] * 2,
-        in_specs=[vmem, vmem, vmem, anywhere, anywhere, vmem, vmem],
+        out_shape=[pltpu.VMEM((groups, HD), jnp.float32)] * 2,
+        in_specs=[vmem] * (2 + len(far)) + [anywhere, anywhere, vmem, vmem],
         out_specs=[vmem] * 2,
         scratch_shapes=[
             pltpu.VMEM((width, width_dev), jnp.bfloat16),
@@ -246,26 +267,32 @@
             pltpu.SemaphoreType.DMA((2,)),
         ],
         name="token",
-    )(token, pair, jnp.stack(far), forget_weight, value_weight, lower_row, new_query)
-    got = pltpu.with_memory_space_constraint(got, pltpu.VMEM)
-    state_cache, shares = pl.pallas_call(
+    )(
+        near(token), near(pair), *map(near, far), forget_weight, value_weight,
+        near(lower_row), near(new_query),
+    )
+    got = near(got)
+    final, shares = pl.pallas_call(
         functools.partial(state_kernel, axis="sp"),
         out_shape=[
-            jax.ShapeDtypeStruct((row_share, head_count, seq_count, HD), jnp.bfloat16),
+            pltpu.VMEM((row_share, head_count, seq_count, HD), jnp.bfloat16),
             pltpu.VMEM((blocks, groups, HD), jnp.float32),
         ],
         in_specs=[vmem, vmem],
         out_specs=[vmem, vmem],
         name="state",
-    )(got, reach)
-    shares = pltpu.with_memory_space_constraint(lax.all_to_all(shares, "sp", 0, 0, tiled=True), pltpu.VMEM)
-    first_read = pl.pallas_call(
+    )(got, near(reach))
+    shares = near(lax.all_to_all(shares, "sp", 0, 0, tiled=True))
+    state_cache, first_read = pl.pallas_call(
         read_kernel,
-        out_shape=jax.ShapeDtypeStruct((seq_count, width_dev), jnp.bfloat16),
-        in_specs=[vmem, vmem, vmem],
-        out_specs=vmem,
+        out_shape=[
+            jax.ShapeDtypeStruct(final.shape, final.dtype),
+            jax.ShapeDtypeStruct((seq_count, width_dev), jnp.bfloat16),
+        ],
+        in_specs=[vmem] * 4,
+        out_specs=[vmem] * 2,
         name="read",
-    )(shares, addend, read_gain[None])
+    )(shares, near(addend), near(read_gain[None]), near(final))
     return (state_cache, first_read)
 
 

time: 61.4 us -> 59.3 us (0.966)
  Pallas kernels: 17.7 us -> 14.3 us
  waiting for transfers between devices: 10.3 us -> 12.2 us
  other arithmetic: 0.63 us -> 0.01 us
    pallas_call x3, Pallas kernels: 8.1 us -> 4.77 us  [the longest x1 2.99 us: local(): pl.pallas_call(functools.partial(token_kernel, axis='tp'), out_shape=[plt...]
    all_to_all x1, waiting for transfers between devices: 7.26 us -> 9.25 us  [local(): got = lax.all_to_all(sent, 'sp', 0, 0, tiled=True)]
    another operation x1 -> x0, other arithmetic: 0.62 us -> none  [local(): jnp.stack(far)]
  transfers between devices with their start and end apart: 5 -> 5, of which waited for: 4 -> 4; matrix products, arithmetic and copies ran while one was open for 1% -> 0% of each run, Pallas kernels for 7% -> 5%
where the time goes in v4:
time: 59.3 us; the launch traced here: 59.1 us
  starting transfers between devices  16.4 us (28%)
  blocking collectives  15.4 us (26%)
  Pallas kernels  14.3 us (24%)
  waiting for transfers between devices  12.2 us (21%)
  between operations  0.72 us (1%)
    all_to_all x1, blocking collectives, local(): shares = near(lax.all_to_all(shares, 'sp', 0, 0, tiled=True))  15.4 us
    all_to_all x1, starting transfers between devices, local(): got = lax.all_to_all(sent, 'sp', 0, 0, tiled=True)  11.5 us
    pallas_call x1, Pallas kernels, local(): pl.pallas_call(dense_kernel, out_shape=jax.ShapeDtypeStruct((blocks, rows...  9.52 us
    all_to_all x1, waiting for transfers between devices, local(): got = lax.all_to_all(sent, 'sp', 0, 0, tiled=True)  9.25 us
    ppermute x3, starting transfers between devices, local(): lax.ppermute(both, 'tp', [(i, (i + 2 * step) % peers) for i in range(peer...  4.83 us
    pallas_call x1, Pallas kernels, local(): pl.pallas_call(functools.partial(token_kernel, axis='tp'), out_shape=[plt...  2.99 us
    ppermute x3, waiting for transfers between devices, local(): lax.ppermute(both, 'tp', [(i, (i + 2 * step) % peers) for i in range(peer...  1.85 us
  transfers between devices with their start and end apart: 5, of which 4 were waited for; matrix products, arithmetic and copies ran while one was open for 0% of the time, Pallas kernels for 5%

profile of v4, /device:TPU:2, one launch (start us, length us, event | category | flops | bytes accessed | tf_op | source)
XLA Modules:
  0.0 59.1 jit_solution(9655295135020426527)
XLA Ops:
  0.6 0.0 copy-start
  0.6 0.0 copy-start.1
  0.7 0.0 copy-start.2
  0.7 9.5 %dense.1 = f32[32,40,128]{2,1,0:T(8,128)} custom-call(bf16[4,192,4096]{2,1,0:T(8,128)(2,1)} %prompt.1, bf16[4096,256]{1,0:T(8,128)(2,1)} %refs_3_.1, bf16[4096,256]{1,0:T(8,128)(2,1)} %refs_4_.1, f32[1,256]{1,0:T(1,128)} %bitcast.6, f32[4,192,256]{2,1,0:T(8,128)} %extra_decay.1), custom_call_target="tpu_custom_call" | custom-call | tf_op jit(solution)/shard_map/dense/pallas_call | solution.py:233
  10.2 11.5 %all-to-all-start = ((f32[32,40,128]{2,1,0:T(8,128)}), f32[32,40,128]{2,1,0:T(8,128)S(1)}, u32[]{:S(2)}, u32[]{:S(2)}) async-start(f32[32,40,128]{2,1,0:T(8,128)} %dense.1), calls=%async_computation | async-start | bytes 1310720 | tf_op jit(solution)/shard_map/all_to_all | solution.py:249
  21.7 0.0 copy-done
  21.7 0.1 collective-permute-start
  21.8 1.2 %collective-permute-done.pair = bf16[4,512]{1,0:T(4,128)(2,1)S(1)} collective-permute-done((bf16[4,512]{1,0:T(4,128)(2,1)S(1)}, bf16[4,512]{1,0:T(4,128)(2,1)S(1)}, u32[]{:S(2)}, u32[]{:S(2)}) %collective-permute-start) | collective-permute-done | bytes 4128 | tf_op jit(solution)/shard_map/ppermute | solution.py:251
  23.0 0.0 copy-start.3
  23.0 0.6 %collective-permute-start.3 = (bf16[2,4,512]{2,1,0:T(4,128)(2,1)S(1)}, bf16[2,4,512]{2,1,0:T(4,128)(2,1)S(1)}, u32[]{:S(2)}, u32[]{:S(2)}) collective-permute-start(bf16[2,4,512]{2,1,0:T(4,128)(2,1)S(1)} %pad_maximum_fusion), channel_id=1, source_target_pairs={{0,6},{1,7},{2,0},{3,1},{4,2},{5,3},{6,4},{7,5},{8,14},{9,15},{10,... | collective-permute-start | bytes 24584 | tf_op jit(solution)/shard_map/ppermute | solution.py:256
  23.6 2.4 %collective-permute-start.2 = (bf16[2,4,512]{2,1,0:T(4,128)(2,1)S(1)}, bf16[2,4,512]{2,1,0:T(4,128)(2,1)S(1)}, u32[]{:S(2)}, u32[]{:S(2)}) collective-permute-start(bf16[2,4,512]{2,1,0:T(4,128)(2,1)S(1)} %pad_maximum_fusion), channel_id=1, source_target_pairs={{0,4},{1,5},{2,6},{3,7},{4,0},{5,1},{6,2},{7,3},{8,12},{9,13},{10,... | collective-permute-start | bytes 24584 | tf_op jit(solution)/shard_map/ppermute | solution.py:256
  26.0 1.8 %collective-permute-start.1 = (bf16[2,4,512]{2,1,0:T(4,128)(2,1)S(1)}, bf16[2,4,512]{2,1,0:T(4,128)(2,1)S(1)}, u32[]{:S(2)}, u32[]{:S(2)}) collective-permute-start(bf16[2,4,512]{2,1,0:T(4,128)(2,1)S(1)} %pad_maximum_fusion), channel_id=1, source_target_pairs={{0,2},{1,3},{2,4},{3,5},{4,6},{5,7},{6,0},{7,1},{8,10},{9,11},{10,... | collective-permute-start | bytes 24584 | tf_op jit(solution)/shard_map/ppermute | solution.py:256
  27.8 0.0 collective-permute-done.3.refs_2_
  27.8 0.9 %collective-permute-done.2.refs_1_ = bf16[2,4,512]{2,1,0:T(4,128)(2,1)S(1)} collective-permute-done((bf16[2,4,512]{2,1,0:T(4,128)(2,1)S(1)}, bf16[2,4,512]{2,1,0:T(4,128)(2,1)S(1)}, u32[]{:S(2)}, u32[]{:S(2)}) %collective-permute-start.2) | collective-permute-done | bytes 8224 | tf_op jit(solution)/shard_map/ppermute | solution.py:256
  28.7 0.9 %collective-permute-done.1.refs_0_ = bf16[2,4,512]{2,1,0:T(4,128)(2,1)S(1)} collective-permute-done((bf16[2,4,512]{2,1,0:T(4,128)(2,1)S(1)}, bf16[2,4,512]{2,1,0:T(4,128)(2,1)S(1)}, u32[]{:S(2)}, u32[]{:S(2)}) %collective-permute-start.1) | collective-permute-done | bytes 8224 | tf_op jit(solution)/shard_map/ppermute | solution.py:256
  29.7 0.0 copy-done.1
  29.7 0.0 copy-done.2
  29.7 3.0 %token_.1 = (f32[8,128]{1,0:T(8,128)S(1)}, f32[8,128]{1,0:T(8,128)S(1)}) custom-call(bf16[4,512]{1,0:T(4,128)(2,1)S(1)} %copy-done, bf16[4,512]{1,0:T(4,128)(2,1)S(1)} %collective-permute-done.pair, bf16[2,4,512]{2,1,0:T(4,128)(2,1)S(1)} %collective-permute-done.1.refs_0_, bf16[2,4,512]{2,1,0:T(4,128)(2,1)S(1)} %collective-permute-done.2.refs_1_, ...), custom_call_target="tpu_custom_call" | custom-call | tf_op jit(solution)/shard_map/token/pallas_call | solution.py:258
  32.7 9.2 %all-to-all-done.got = f32[32,40,128]{2,1,0:T(8,128)S(1)} async-done(((f32[32,40,128]{2,1,0:T(8,128)}), f32[32,40,128]{2,1,0:T(8,128)S(1)}, u32[]{:S(2)}, u32[]{:S(2)}) %all-to-all-start) | async-done | bytes 655392 | tf_op jit(solution)/shard_map/all_to_all | solution.py:249
  41.9 1.1 %state.1 = (bf16[4,2,4,128]{3,2,1,0:T(4,128)(2,1)S(1)}, f32[32,8,128]{2,1,0:T(8,128)S(1)}) custom-call(f32[32,40,128]{2,1,0:T(8,128)S(1)} %all-to-all-done.got, f32[8,128]{1,0:T(8,128)S(1)} %get-tuple-element.8.reach), custom_call_target="tpu_custom_call" | custom-call | tf_op jit(solution)/shard_map/state/pallas_call | solution.py:275
  43.0 15.4 %all_to_all.10.shares = f32[32,8,128]{2,1,0:T(8,128)S(1)} all-to-all(f32[32,8,128]{2,1,0:T(8,128)S(1)} %get-tuple-element.9), channel_id=1, replica_groups=mesh['sp'=32,'tp'=8] {'sp'}, dimensions={0} | all-to-all | bytes 262144 | tf_op jit(solution)/shard_map/all_to_all | solution.py:285
  58.4 0.0 copy-done.3
  58.4 0.7 %read.1 = (bf16[4,2,4,128]{3,2,1,0:T(4,128)(2,1)}, bf16[4,256]{1,0:T(4,128)(2,1)}) custom-call(f32[32,8,128]{2,1,0:T(8,128)S(1)} %all_to_all.10.shares, f32[8,128]{1,0:T(8,128)S(1)} %get-tuple-element.10.addend, f32[1,128]{1,0:T(1,128)S(1)} %bitcast.8, bf16[4,2,4,128]{3,2,1,0:T(4,128)(2,1)S(1)} %get-tuple-element.11.final), custom_call_target="tpu_custom_call" | custom-call | tf_op jit(solution)/shard_map/read/pallas_call | solution.py:286
  (1 shorter events, 0.0 us)
Async XLA Ops:
  0.6 21.1 %copy-start = (bf16[4,512]{1,0:T(4,128)(2,1)S(1)}, bf16[4,512]{1,0:T(4,128)(2,1)}, u32[]{:S(2)}) copy-start(bf16[4,512]{1,0:T(4,128)(2,1)} %own) | copy-start | bytes 12292
  0.6 29.0 %copy-start.1 = (f32[256]{0:T(256)S(1)}, f32[256]{0:T(256)}, u32[]{:S(2)}) copy-start(f32[256]{0:T(256)} %param.11) | copy-start | bytes 3076
  0.7 29.0 %copy-start.2 = (bf16[4,256]{1,0:T(4,128)(2,1)S(1)}, bf16[4,256]{1,0:T(4,128)(2,1)}, u32[]{:S(2)}) copy-start(bf16[4,256]{1,0:T(4,128)(2,1)} %refs_6_.1) | copy-start | bytes 6148
  10.2 31.7 %all-to-all-start = ((f32[32,40,128]{2,1,0:T(8,128)}), f32[32,40,128]{2,1,0:T(8,128)S(1)}, u32[]{:S(2)}, u32[]{:S(2)}) async-start(f32[32,40,128]{2,1,0:T(8,128)} %dense.1), calls=%async_computation | async-start | bytes 1310720 | tf_op jit(solution)/shard_map/all_to_all | solution.py:249
  21.7 1.3 %collective-permute-start = (bf16[4,512]{1,0:T(4,128)(2,1)S(1)}, bf16[4,512]{1,0:T(4,128)(2,1)S(1)}, u32[]{:S(2)}, u32[]{:S(2)}) collective-permute-start(bf16[4,512]{1,0:T(4,128)(2,1)S(1)} %copy-done), channel_id=1, source_target_pairs={{0,1},{1,0},{2,3},{3,2},{4,5},{5,4},{6,7},{7,6},{8,9},{9,8},{10,11... | collective-permute-start | bytes 12296 | tf_op jit(solution)/shard_map/ppermute | solution.py:251
  23.0 35.4 %copy-start.3 = (f32[128]{0:T(128)S(1)}, f32[128]{0:T(128)}, u32[]{:S(2)}) copy-start(f32[128]{0:T(128)} %param.15) | copy-start | bytes 1540
  23.0 4.8 %collective-permute-start.3 = (bf16[2,4,512]{2,1,0:T(4,128)(2,1)S(1)}, bf16[2,4,512]{2,1,0:T(4,128)(2,1)S(1)}, u32[]{:S(2)}, u32[]{:S(2)}) collective-permute-start(bf16[2,4,512]{2,1,0:T(4,128)(2,1)S(1)} %pad_maximum_fusion), channel_id=1, source_target_pairs={{0,6},{1,7},{2,0},{3,1},{4,2},{5,3},{6,4},{7,5},{8,14},{9,15},{10,... | collective-permute-start | bytes 24584 | tf_op jit(solution)/shard_map/ppermute | solution.py:256
  23.6 5.2 %collective-permute-start.2 = (bf16[2,4,512]{2,1,0:T(4,128)(2,1)S(1)}, bf16[2,4,512]{2,1,0:T(4,128)(2,1)S(1)}, u32[]{:S(2)}, u32[]{:S(2)}) collective-permute-start(bf16[2,4,512]{2,1,0:T(4,128)(2,1)S(1)} %pad_maximum_fusion), channel_id=1, source_target_pairs={{0,4},{1,5},{2,6},{3,7},{4,0},{5,1},{6,2},{7,3},{8,12},{9,13},{10,... | collective-permute-start | bytes 24584 | tf_op jit(solution)/shard_map/ppermute | solution.py:256
  26.0 3.7 %collective-permute-start.1 = (bf16[2,4,512]{2,1,0:T(4,128)(2,1)S(1)}, bf16[2,4,512]{2,1,0:T(4,128)(2,1)S(1)}, u32[]{:S(2)}, u32[]{:S(2)}) collective-permute-start(bf16[2,4,512]{2,1,0:T(4,128)(2,1)S(1)} %pad_maximum_fusion), channel_id=1, source_target_pairs={{0,2},{1,3},{2,4},{3,5},{4,6},{5,7},{6,0},{7,1},{8,10},{9,11},{10,... | collective-permute-start | bytes 24584 | tf_op jit(solution)/shard_map/ppermute | solution.py:256

commit v5 on v4

--- a/solution.py
+++ b/solution.py
@@ -74,6 +74,9 @@
     row = lax.broadcasted_iota(jnp.int32, (span_len, span_len), 0)
     col = lax.broadcasted_iota(jnp.int32, (span_len, span_len), 1)
     after = jnp.where(col > row, 1.0, 0.0).astype(jnp.bfloat16)
+
+    lane = lax.broadcasted_iota(jnp.int32, (HD, HD), 1)
+    powers = [jnp.zeros((HD, HD), jnp.float32)]
 
     def finish(s, opening, forget_pre, values):
         key = key_of(forget_pre.astype(jnp.float32), opening)
@@ -97,6 +100,10 @@
                 weighted[:, cut], values[:, cut], (((0,), (0,)), ((), ())),
                 preferred_element_type=jnp.float32,
             )
+            peak = jnp.max(jnp.abs(state), axis=1, keepdims=True)
+            power = jnp.ceil(jnp.log2(jnp.maximum(peak, 1e-30)))
+            state = state * jnp.exp2(-power)
+            powers[0] = jnp.where(lane == group, power, powers[0])
             for k in range(dests):
                 sent[k, pl.ds(group, row_share, stride=groups), :] = state[
                     k * row_share : (k + 1) * row_share
@@ -125,8 +132,18 @@
         finish(s - 1, opening, *pending)
         pending = (forget_pre, values)
     finish(seq_count - 1, opening, *pending)
+    total = tot[...]
+    high = total.astype(jnp.bfloat16).astype(jnp.float32)
+    left = total - high
+    middle = left.astype(jnp.bfloat16).astype(jnp.float32)
+    parts = (high, middle, left - middle, powers[0].T[:groups])
+    at = lax.broadcasted_iota(jnp.int32, (groups, HD), 1) // row_share
     for k in range(dests):
-        sent[k, row_share * groups :, :] = tot[...]
+        tile = None
+        for i, part in enumerate(parts):
+            turned = pltpu.roll(part, (HD + (i - k) * row_share) % HD, 1)
+            tile = turned if tile is None else jnp.where(at == i, turned, tile)
+        sent[k, row_share * groups :, :] = tile
 
 
 def token_kernel(
@@ -170,26 +187,29 @@
     addend[...] = key_sum * grouped(rounded(value_w))
 
 
-def state_kernel(got, reach, state_cache, shares, *, axis):
+def state_kernel(got, reach, final_out, shares, *, axis):
     blocks, _, _ = got.shape
     groups = reach.shape[0]
     row_share = HD // blocks
-    head_count, seq_count = state_cache.shape[1:3]
-    back = lax.rem(HD - lax.axis_index(axis) * row_share, HD)
+    head_count, seq_count = final_out.shape[1:3]
     final = [None] * row_share
     later = jnp.zeros((groups, HD), jnp.float32)
     for b in range(blocks - 1, -1, -1):
-        scale = pltpu.roll(jnp.exp(later), back, 1)
+        tile = got[b, row_share * groups :, :]
+        middle, low, power = (
+            pltpu.roll(tile, HD - i * row_share, 1) for i in range(1, 4)
+        )
+        scale = jnp.exp(later) * jnp.exp2(power)
         for d in range(row_share):
             term = scale[:, d : d + 1] * got[b, d * groups : (d + 1) * groups, :]
             final[d] = term if final[d] is None else final[d] + term
-        if b > 0:
-            later = later + got[b, row_share * groups :, :]
+        later = later + (tile + (middle + low))
+    back = lax.rem(HD - lax.axis_index(axis) * row_share, HD)
     own_reach = pltpu.roll(reach[...], back, 1)
     share = None
     for d in range(row_share):
         for h in range(head_count):
-            state_cache[d, h] = final[d][h * seq_count : (h + 1) * seq_count].astype(jnp.bfloat16)
+            final_out[d, h] = final[d][h * seq_count : (h + 1) * seq_count].astype(jnp.bfloat16)
         term = own_reach[:, d : d + 1] * final[d]
         share = term if share is None else share + term
     for k in range(blocks):
@@ -230,9 +250,10 @@
     anywhere = pl.BlockSpec(memory_space=pltpu.HBM)
     vmem = pl.BlockSpec(memory_space=pltpu.VMEM)
     lower_row = lower_bound[None]
+    pair = lax.ppermute(new_token, "tp", [(i, i ^ 1) for i in range(peers)])
     sent = pl.pallas_call(
         dense_kernel,
-        out_shape=jax.ShapeDtypeStruct((blocks, rows, HD), jnp.float32),
+        out_shape=pltpu.VMEM((blocks, rows, HD), jnp.float32),
         in_specs=[anywhere] * 5,
         out_specs=vmem,
         scratch_shapes=[
@@ -246,9 +267,9 @@
         ],
         name="dense",
     )(prompt, forget_weight, value_weight, lower_row, extra_decay)
+    sent = sent.astype(jnp.float16)
     got = lax.all_to_all(sent, "sp", 0, 0, tiled=True)
-    token, _ = lax.optimization_barrier((new_token, sent))
-    pair = lax.ppermute(token, "tp", [(i, i ^ 1) for i in range(peers)])
+    token, pair, _ = lax.optimization_barrier((new_token, pair, sent))
     both = jnp.stack([token, pair])
     far = []
     for step in range(1, peers // 2):
@@ -271,7 +292,7 @@
         near(token), near(pair), *map(near, far), forget_weight, value_weight,
         near(lower_row), near(new_query),
     )
-    got = near(got)
+    got = near(got.astype(jnp.float32))
     final, shares = pl.pallas_call(
         functools.partial(state_kernel, axis="sp"),
         out_shape=[

time: 59.3 us -> 55.9 us (0.943); the launches traced: 59.1 us -> 55 us
  waiting for transfers between devices: 12.2 us -> 6.1 us
  blocking collectives: 15.4 us -> 17.1 us
  other arithmetic: 0.01 us -> 0.82 us
    all_to_all x1, waiting for transfers between devices: 9.25 us -> 3.1 us  [local(): got = lax.all_to_all(sent, 'sp', 0, 0, tiled=True)]
    all_to_all x1, blocking collectives: 15.4 us -> 17.1 us  [local(): shares = near(lax.all_to_all(shares, 'sp', 0, 0, tiled=True))]
    convert_element_type x0 -> x2, other arithmetic: none -> 0.81 us  [the longest x1 0.77 us: local(): sent = sent.astype(jnp.float16)]
where the time goes in v5:
time: 55.9 us; the launch traced here: 55 us
  blocking collectives  17.1 us (31%)
  starting transfers between devices  16.4 us (29%)
  Pallas kernels  13.8 us (25%)
  waiting for transfers between devices  6.1 us (11%)
  other arithmetic  0.82 us (1%)
  between operations  0.72 us (1%)
    all_to_all x1, blocking collectives, local(): shares = near(lax.all_to_all(shares, 'sp', 0, 0, tiled=True))  17.1 us
    all_to_all x1, starting transfers between devices, local(): got = lax.all_to_all(sent, 'sp', 0, 0, tiled=True)  11.5 us
    pallas_call x1, Pallas kernels, local(): pl.pallas_call(dense_kernel, out_shape=pltpu.VMEM((blocks, rows, HD), jnp...  9.1 us
    ppermute x3, starting transfers between devices, local(): lax.ppermute(both, 'tp', [(i, (i + 2 * step) % peers) for i in range(peer...  4.84 us
    all_to_all x1, waiting for transfers between devices, local(): got = lax.all_to_all(sent, 'sp', 0, 0, tiled=True)  3.1 us
    pallas_call x1, Pallas kernels, local(): pl.pallas_call(functools.partial(token_kernel, axis='tp'), out_shape=[plt...  2.99 us
    ppermute x3, waiting for transfers between devices, local(): lax.ppermute(both, 'tp', [(i, (i + 2 * step) % peers) for i in range(peer...  1.84 us
    ppermute x1, waiting for transfers between devices, local(): pair = lax.ppermute(new_token, 'tp', [(i, i ^ 1) for i in range(peers)])  1.15 us
  transfers between devices with their start and end apart: 5, of which 4 were waited for; matrix products, arithmetic and copies ran while one was open for 0% of the time, Pallas kernels for 5%

profile of v5, /device:TPU:2, one launch (start us, length us, event | category | flops | bytes accessed | tf_op | source)
XLA Modules:
  0.0 55.0 jit_solution(1685101761877572707)
XLA Ops:
  0.6 0.0 copy-start
  0.6 0.0 copy-start.1
  0.7 0.0 copy-start.2
  0.7 9.1 %dense.1 = f32[32,40,128]{2,1,0:T(8,128)S(1)} custom-call(bf16[4,192,4096]{2,1,0:T(8,128)(2,1)} %prompt.1, bf16[4096,256]{1,0:T(8,128)(2,1)} %refs_3_.1, bf16[4096,256]{1,0:T(8,128)(2,1)} %refs_4_.1, f32[1,256]{1,0:T(1,128)} %bitcast.6, f32[4,192,256]{2,1,0:T(8,128)} %extra_decay.1), custom_call_target="tpu_custom_call" | custom-call | tf_op jit(solution)/shard_map/dense/pallas_call | solution.py:254
  9.8 0.8 %convert_element_type.6 = f16[32,40,128]{2,1,0:T(8,128)(2,1)} convert(f32[32,40,128]{2,1,0:T(8,128)S(1)} %dense.1) | non-fusion elementwise | flops 163840 | bytes 983040 | tf_op jit(solution)/shard_map/convert_element_type | solution.py:270
  10.5 11.5 %all-to-all-start = ((f16[32,40,128]{2,1,0:T(8,128)(2,1)}), f16[32,40,128]{2,1,0:T(8,128)(2,1)S(1)}, u32[]{:S(2)}, u32[]{:S(2)}) async-start(f16[32,40,128]{2,1,0:T(8,128)(2,1)} %convert_element_type.6), calls=%async_computation | async-start | bytes 655360 | tf_op jit(solution)/shard_map/all_to_all | solution.py:271
  22.0 0.0 copy-done
  22.0 0.1 collective-permute-start
  22.1 1.2 %collective-permute-done.pair = bf16[4,512]{1,0:T(4,128)(2,1)S(1)} collective-permute-done((bf16[4,512]{1,0:T(4,128)(2,1)S(1)}, bf16[4,512]{1,0:T(4,128)(2,1)S(1)}, u32[]{:S(2)}, u32[]{:S(2)}) %collective-permute-start) | collective-permute-done | bytes 4128 | tf_op jit(solution)/shard_map/ppermute | solution.py:253
  23.3 0.0 copy-start.3
  23.3 0.6 %collective-permute-start.3 = (bf16[2,4,512]{2,1,0:T(4,128)(2,1)S(1)}, bf16[2,4,512]{2,1,0:T(4,128)(2,1)S(1)}, u32[]{:S(2)}, u32[]{:S(2)}) collective-permute-start(bf16[2,4,512]{2,1,0:T(4,128)(2,1)S(1)} %pad_maximum_fusion), channel_id=1, source_target_pairs={{0,6},{1,7},{2,0},{3,1},{4,2},{5,3},{6,4},{7,5},{8,14},{9,15},{10,... | collective-permute-start | bytes 24584 | tf_op jit(solution)/shard_map/ppermute | solution.py:277
  23.9 2.4 %collective-permute-start.2 = (bf16[2,4,512]{2,1,0:T(4,128)(2,1)S(1)}, bf16[2,4,512]{2,1,0:T(4,128)(2,1)S(1)}, u32[]{:S(2)}, u32[]{:S(2)}) collective-permute-start(bf16[2,4,512]{2,1,0:T(4,128)(2,1)S(1)} %pad_maximum_fusion), channel_id=1, source_target_pairs={{0,4},{1,5},{2,6},{3,7},{4,0},{5,1},{6,2},{7,3},{8,12},{9,13},{10,... | collective-permute-start | bytes 24584 | tf_op jit(solution)/shard_map/ppermute | solution.py:277
  26.4 1.8 %collective-permute-start.1 = (bf16[2,4,512]{2,1,0:T(4,128)(2,1)S(1)}, bf16[2,4,512]{2,1,0:T(4,128)(2,1)S(1)}, u32[]{:S(2)}, u32[]{:S(2)}) collective-permute-start(bf16[2,4,512]{2,1,0:T(4,128)(2,1)S(1)} %pad_maximum_fusion), channel_id=1, source_target_pairs={{0,2},{1,3},{2,4},{3,5},{4,6},{5,7},{6,0},{7,1},{8,10},{9,11},{10,... | collective-permute-start | bytes 24584 | tf_op jit(solution)/shard_map/ppermute | solution.py:277
  28.2 0.0 collective-permute-done.3.refs_2_
  28.2 0.9 %collective-permute-done.2.refs_1_ = bf16[2,4,512]{2,1,0:T(4,128)(2,1)S(1)} collective-permute-done((bf16[2,4,512]{2,1,0:T(4,128)(2,1)S(1)}, bf16[2,4,512]{2,1,0:T(4,128)(2,1)S(1)}, u32[]{:S(2)}, u32[]{:S(2)}) %collective-permute-start.2) | collective-permute-done | bytes 8224 | tf_op jit(solution)/shard_map/ppermute | solution.py:277
  29.1 0.9 %collective-permute-done.1.refs_0_ = bf16[2,4,512]{2,1,0:T(4,128)(2,1)S(1)} collective-permute-done((bf16[2,4,512]{2,1,0:T(4,128)(2,1)S(1)}, bf16[2,4,512]{2,1,0:T(4,128)(2,1)S(1)}, u32[]{:S(2)}, u32[]{:S(2)}) %collective-permute-start.1) | collective-permute-done | bytes 8224 | tf_op jit(solution)/shard_map/ppermute | solution.py:277
  30.0 0.0 copy-done.1
  30.0 0.0 copy-done.2
  30.0 3.0 %token_.1 = (f32[8,128]{1,0:T(8,128)S(1)}, f32[8,128]{1,0:T(8,128)S(1)}) custom-call(bf16[4,512]{1,0:T(4,128)(2,1)S(1)} %copy-done, bf16[4,512]{1,0:T(4,128)(2,1)S(1)} %collective-permute-done.pair, bf16[2,4,512]{2,1,0:T(4,128)(2,1)S(1)} %collective-permute-done.1.refs_0_, bf16[2,4,512]{2,1,0:T(4,128)(2,1)S(1)} %collective-permute-done.2.refs_1_, ...), custom_call_target="tpu_custom_call" | custom-call | tf_op jit(solution)/shard_map/token/pallas_call | solution.py:279
  33.0 3.1 %all-to-all-done = f16[32,40,128]{2,1,0:T(8,128)(2,1)S(1)} async-done(((f16[32,40,128]{2,1,0:T(8,128)(2,1)}), f16[32,40,128]{2,1,0:T(8,128)(2,1)S(1)}, u32[]{:S(2)}, u32[]{:S(2)}) %all-to-all-start) | async-done | bytes 327712 | tf_op jit(solution)/shard_map/all_to_all | solution.py:271
  36.2 1.0 %state.1 = (bf16[4,2,4,128]{3,2,1,0:T(4,128)(2,1)S(1)}, f32[32,8,128]{2,1,0:T(8,128)S(1)}) custom-call(f32[32,40,128]{2,1,0:T(8,128)S(1)} %convert_element_type.7.got, f32[8,128]{1,0:T(8,128)S(1)} %get-tuple-element.10.reach), custom_call_target="tpu_custom_call" | custom-call | tf_op jit(solution)/shard_map/state/pallas_call | solution.py:296
  37.2 17.1 %all_to_all.10.shares = f32[32,8,128]{2,1,0:T(8,128)S(1)} all-to-all(f32[32,8,128]{2,1,0:T(8,128)S(1)} %get-tuple-element.11), channel_id=1, replica_groups=mesh['sp'=32,'tp'=8] {'sp'}, dimensions={0} | all-to-all | bytes 262144 | tf_op jit(solution)/shard_map/all_to_all | solution.py:306
  54.3 0.0 copy-done.3
  54.3 0.7 %read.1 = (bf16[4,2,4,128]{3,2,1,0:T(4,128)(2,1)}, bf16[4,256]{1,0:T(4,128)(2,1)}) custom-call(f32[32,8,128]{2,1,0:T(8,128)S(1)} %all_to_all.10.shares, f32[8,128]{1,0:T(8,128)S(1)} %get-tuple-element.12.addend, f32[1,128]{1,0:T(1,128)S(1)} %bitcast.8, bf16[4,2,4,128]{3,2,1,0:T(4,128)(2,1)S(1)} %get-tuple-element.13.final), custom_call_target="tpu_custom_call" | custom-call | tf_op jit(solution)/shard_map/read/pallas_call | solution.py:307
  (2 shorter events, 0.1 us)
Async XLA Ops:
  0.6 21.4 %copy-start = (bf16[4,512]{1,0:T(4,128)(2,1)S(1)}, bf16[4,512]{1,0:T(4,128)(2,1)}, u32[]{:S(2)}) copy-start(bf16[4,512]{1,0:T(4,128)(2,1)} %own) | copy-start | bytes 12292
  0.6 29.4 %copy-start.1 = (f32[256]{0:T(256)S(1)}, f32[256]{0:T(256)}, u32[]{:S(2)}) copy-start(f32[256]{0:T(256)} %param.11) | copy-start | bytes 3076
  0.7 29.4 %copy-start.2 = (bf16[4,256]{1,0:T(4,128)(2,1)S(1)}, bf16[4,256]{1,0:T(4,128)(2,1)}, u32[]{:S(2)}) copy-start(bf16[4,256]{1,0:T(4,128)(2,1)} %refs_6_.1) | copy-start | bytes 6148
  10.5 25.6 %all-to-all-start = ((f16[32,40,128]{2,1,0:T(8,128)(2,1)}), f16[32,40,128]{2,1,0:T(8,128)(2,1)S(1)}, u32[]{:S(2)}, u32[]{:S(2)}) async-start(f16[32,40,128]{2,1,0:T(8,128)(2,1)} %convert_element_type.6), calls=%async_computation | async-start | bytes 655360 | tf_op jit(solution)/shard_map/all_to_all | solution.py:271
  22.0 1.3 %collective-permute-start = (bf16[4,512]{1,0:T(4,128)(2,1)S(1)}, bf16[4,512]{1,0:T(4,128)(2,1)S(1)}, u32[]{:S(2)}, u32[]{:S(2)}) collective-permute-start(bf16[4,512]{1,0:T(4,128)(2,1)S(1)} %copy-done), channel_id=1, source_target_pairs={{0,1},{1,0},{2,3},{3,2},{4,5},{5,4},{6,7},{7,6},{8,9},{9,8},{10,11... | collective-permute-start | bytes 12296 | tf_op jit(solution)/shard_map/ppermute | solution.py:253
  23.3 31.0 %copy-start.3 = (f32[128]{0:T(128)S(1)}, f32[128]{0:T(128)}, u32[]{:S(2)}) copy-start(f32[128]{0:T(128)} %param.15) | copy-start | bytes 1540
  23.3 4.8 %collective-permute-start.3 = (bf16[2,4,512]{2,1,0:T(4,128)(2,1)S(1)}, bf16[2,4,512]{2,1,0:T(4,128)(2,1)S(1)}, u32[]{:S(2)}, u32[]{:S(2)}) collective-permute-start(bf16[2,4,512]{2,1,0:T(4,128)(2,1)S(1)} %pad_maximum_fusion), channel_id=1, source_target_pairs={{0,6},{1,7},{2,0},{3,1},{4,2},{5,3},{6,4},{7,5},{8,14},{9,15},{10,... | collective-permute-start | bytes 24584 | tf_op jit(solution)/shard_map/ppermute | solution.py:277
  23.9 5.2 %collective-permute-start.2 = (bf16[2,4,512]{2,1,0:T(4,128)(2,1)S(1)}, bf16[2,4,512]{2,1,0:T(4,128)(2,1)S(1)}, u32[]{:S(2)}, u32[]{:S(2)}) collective-permute-start(bf16[2,4,512]{2,1,0:T(4,128)(2,1)S(1)} %pad_maximum_fusion), channel_id=1, source_target_pairs={{0,4},{1,5},{2,6},{3,7},{4,0},{5,1},{6,2},{7,3},{8,12},{9,13},{10,... | collective-permute-start | bytes 24584 | tf_op jit(solution)/shard_map/ppermute | solution.py:277
  26.4 3.7 %collective-permute-start.1 = (bf16[2,4,512]{2,1,0:T(4,128)(2,1)S(1)}, bf16[2,4,512]{2,1,0:T(4,128)(2,1)S(1)}, u32[]{:S(2)}, u32[]{:S(2)}) collective-permute-start(bf16[2,4,512]{2,1,0:T(4,128)(2,1)S(1)} %pad_maximum_fusion), channel_id=1, source_target_pairs={{0,2},{1,3},{2,4},{3,5},{4,6},{5,7},{6,0},{7,1},{8,10},{9,11},{10,... | collective-permute-start | bytes 24584 | tf_op jit(solution)/shard_map/ppermute | solution.py:277

commit v6 on v5

--- a/solution.py
+++ b/solution.py
@@ -146,45 +146,81 @@
         sent[k, row_share * groups :, :] = tile
 
 
-def token_kernel(
-    own, pair, *refs, axis
+def chunk_of(weight, chip, step, chips):
+    rows = weight.shape[0] // chips
+    source = lax.rem(chip + chips - step, chips)
+    return weight.at[pl.ds(pl.multiple_of(source * rows, rows), rows)]
+
+
+def token_start_kernel(
+    own, pair, forget_weight, value_weight, sums, forget_w, forget_own, value_own, sems, *, axis
 ):
-    far = refs[:-10]
-    forget_weight, value_weight, lower_bound, new_query, reach, addend = refs[-10:-4]
-    forget_w, value_w, whole, sems = refs[-4:]
+    me = lax.axis_index(axis)
+    chips = forget_w.shape[0] + 1
+    chip = me // 2
     copies = [
-        pltpu.make_async_copy(forget_weight, forget_w, sems.at[0]),
-        pltpu.make_async_copy(value_weight, value_w, sems.at[1]),
+        pltpu.make_async_copy(chunk_of(forget_weight, chip, 0, chips), forget_own, sems.at[0]),
+        pltpu.make_async_copy(chunk_of(value_weight, chip, 0, chips), value_own, sems.at[1]),
+    ]
+    for step in range(1, chips):
+        copies.append(
+            pltpu.make_async_copy(
+                chunk_of(forget_weight, chip, step, chips), forget_w.at[step - 1],
+                sems.at[step + 1],
+            )
+        )
+    for copy in copies:
+        copy.start()
+    first, second = own[...].astype(jnp.float32), pair[...].astype(jnp.float32)
+    even = lax.rem(me, 2) == 0
+    token = jnp.concatenate(
+        [jnp.where(even, first, second), jnp.where(even, second, first)], axis=1
+    ).astype(jnp.bfloat16)
+    for i, weight in enumerate((forget_own, value_own)):
+        copies[i].wait()
+        sums[i] = jnp.dot(token, weight[...], preferred_element_type=jnp.float32)
+    for copy in copies[2:]:
+        copy.wait()
+
+
+def token_kernel(*refs, axis):
+    far = refs[:-9]
+    sums, forget_w, value_weight, lower_bound, new_query, reach, addend = refs[-9:-2]
+    value_w, sems = refs[-2:]
+    head_count = forget_w.shape[2] // HD
+    me = lax.axis_index(axis)
+    chips = forget_w.shape[0] + 1
+    copies = [
+        pltpu.make_async_copy(
+            chunk_of(value_weight, me // 2, step, chips), value_w.at[step - 1], sems.at[step - 1]
+        )
+        for step in range(1, chips)
     ]
     for copy in copies:
         copy.start()
-    _, part = own.shape
-    peers = whole.shape[1] // part
-    head_count = forget_w.shape[1] // HD
-    me = lax.axis_index(axis)
-    held = [(me, own[...]), (me ^ 1, pair[...])]
-    for step in range(1, peers // 2):
-        source = lax.rem(me + peers - 2 * step, peers)
-        held += [(source, far[step - 1][0]), (source ^ 1, far[step - 1][1])]
-    for source, rows in held:
-        whole[:, pl.ds(pl.multiple_of(source * part, part), part)] = rows.astype(jnp.float32)
-    token = whole[...].astype(jnp.bfloat16)
-    for copy in copies:
-        copy.wait()
+    even = lax.rem(me, 2) == 0
+    tokens = []
+    for pieces in far:
+        first, second = (pieces[i].astype(jnp.float32) for i in (0, 1))
+        tokens += [jnp.where(even, first, second), jnp.where(even, second, first)]
+    token = jnp.concatenate(tokens, axis=1).astype(jnp.bfloat16)
 
     def grouped(rows):
         return jnp.concatenate([rows[:, h * HD : (h + 1) * HD] for h in range(head_count)], axis=0)
 
-    def rounded(weight):
-        out = jnp.dot(token, weight[...], preferred_element_type=jnp.float32)
+    def rounded(i, weight):
+        weight = weight[...].reshape(token.shape[1], weight.shape[2])
+        out = sums[i] + jnp.dot(token, weight, preferred_element_type=jnp.float32)
         return out.astype(jnp.bfloat16).astype(jnp.float32)
 
-    new_key = key_of(rounded(forget_w), 1.0 - lower_bound[...])
+    new_key = key_of(rounded(0, forget_w), 1.0 - lower_bound[...])
     query = new_query[...].astype(jnp.float32)
     query = query / (1.0 + jnp.exp(-query))
     reach[...] = grouped(query * (1.0 - new_key))
     key_sum = jnp.sum(grouped(query * new_key), axis=1, keepdims=True)
-    addend[...] = key_sum * grouped(rounded(value_w))
+    for copy in copies:
+        copy.wait()
+    addend[...] = key_sum * grouped(rounded(1, value_w))
 
 
 def state_kernel(got, reach, final_out, shares, *, axis):
@@ -273,24 +309,37 @@
     both = jnp.stack([token, pair])
     far = []
     for step in range(1, peers // 2):
-        far.append(
-            lax.ppermute(both, "tp", [(i, (i + 2 * step) % peers) for i in range(peers)])
-        )
+        far.append(lax.ppermute(both, "tp", [(i, (i + 2 * step) % peers) for i in range(peers)]))
+    others = len(far)
+    part = width // (others + 1)
+    sums, forget_far = pl.pallas_call(
+        functools.partial(token_start_kernel, axis="tp"),
+        out_shape=[
+            pltpu.VMEM((2, seq_count, width_dev), jnp.float32),
+            pltpu.VMEM((others, part, width_dev), jnp.bfloat16),
+        ],
+        in_specs=[vmem, vmem, anywhere, anywhere],
+        out_specs=[vmem] * 2,
+        scratch_shapes=[
+            pltpu.VMEM((part, width_dev), jnp.bfloat16),
+            pltpu.VMEM((part, width_dev), jnp.bfloat16),
+            pltpu.SemaphoreType.DMA((others + 2,)),
+        ],
+        name="prepare",
+    )(near(token), near(pair), forget_weight, value_weight)
     reach, addend = pl.pallas_call(
         functools.partial(token_kernel, axis="tp"),
         out_shape=[pltpu.VMEM((groups, HD), jnp.float32)] * 2,
-        in_specs=[vmem] * (2 + len(far)) + [anywhere, anywhere, vmem, vmem],
+        in_specs=[vmem] * (others + 2) + [anywhere, vmem, vmem],
         out_specs=[vmem] * 2,
         scratch_shapes=[
-            pltpu.VMEM((width, width_dev), jnp.bfloat16),
-            pltpu.VMEM((width, width_dev), jnp.bfloat16),
-            pltpu.VMEM((seq_count, width), jnp.float32),
-            pltpu.SemaphoreType.DMA((2,)),
+            pltpu.VMEM((others, part, width_dev), jnp.bfloat16),
+            pltpu.SemaphoreType.DMA((others,)),
         ],
         name="token",
     )(
-        near(token), near(pair), *map(near, far), forget_weight, value_weight,
-        near(lower_row), near(new_query),
+        *map(near, far), near(sums), near(forget_far), value_weight, near(lower_row),
+        near(new_query),
     )
     got = near(got.astype(jnp.float32))
     final, shares = pl.pallas_call(

time: 55.9 us -> 55.1 us (0.986)
  the two profiles are of different devices: /device:TPU:2 before, /device:TPU:6 now
where the time goes in v6:
time: 55.1 us; the launch traced here: 54.9 us
  blocking collectives  17.5 us (32%)
  starting transfers between devices  14.6 us (26%)
  Pallas kernels  14.3 us (26%)
  waiting for transfers between devices  6.92 us (13%)
  other arithmetic  0.82 us (1%)
  between operations  0.73 us (1%)
    all_to_all x1, blocking collectives, local(): shares = near(lax.all_to_all(shares, 'sp', 0, 0, tiled=True))  17.5 us
    all_to_all x1, starting transfers between devices, local(): got = lax.all_to_all(sent, 'sp', 0, 0, tiled=True)  11.5 us
    pallas_call x1, Pallas kernels, local(): pl.pallas_call(dense_kernel, out_shape=pltpu.VMEM((blocks, rows, HD), jnp...  8.61 us
    ppermute x3, waiting for transfers between devices, local(): lax.ppermute(both, 'tp', [(i, (i + 2 * step) % peers) for i in range(peer...  3.12 us
    ppermute x3, starting transfers between devices, local(): lax.ppermute(both, 'tp', [(i, (i + 2 * step) % peers) for i in range(peer...  2.98 us
    all_to_all x1, waiting for transfers between devices, local(): got = lax.all_to_all(sent, 'sp', 0, 0, tiled=True)  2.64 us
    pallas_call x1, Pallas kernels, local(): pl.pallas_call(functools.partial(token_kernel, axis='tp'), out_shape=[plt...  2.27 us
    pallas_call x1, Pallas kernels, local(): pl.pallas_call(functools.partial(token_start_kernel, axis='tp'), out_shap...  1.72 us
  transfers between devices with their start and end apart: 5, of which 4 were waited for; matrix products, arithmetic and copies ran while one was open for 0% of the time, Pallas kernels for 7%

profile of v6, /device:TPU:6, one launch (start us, length us, event | category | flops | bytes accessed | tf_op | source)
XLA Modules:
  0.0 54.9 jit_solution(16226102041085394787)
XLA Ops:
  0.6 0.0 copy-start
  0.6 8.6 %dense.1 = f32[32,40,128]{2,1,0:T(8,128)S(1)} custom-call(bf16[4,192,4096]{2,1,0:T(8,128)(2,1)} %prompt.1, bf16[4096,256]{1,0:T(8,128)(2,1)} %forget_weight.3, bf16[4096,256]{1,0:T(8,128)(2,1)} %refs_5_.1, f32[1,256]{1,0:T(1,128)} %bitcast.6, f32[4,192,256]{2,1,0:T(8,128)} %extra_decay.1), custom_call_target="tpu_custom_call" | custom-call | tf_op jit(solution)/shard_map/dense/pallas_call | solution.py:290
  9.3 0.8 %convert_element_type.6 = f16[32,40,128]{2,1,0:T(8,128)(2,1)} convert(f32[32,40,128]{2,1,0:T(8,128)S(1)} %dense.1) | non-fusion elementwise | flops 163840 | bytes 983040 | tf_op jit(solution)/shard_map/convert_element_type | solution.py:306
  10.0 11.5 %all-to-all-start = ((f16[32,40,128]{2,1,0:T(8,128)(2,1)}), f16[32,40,128]{2,1,0:T(8,128)(2,1)S(1)}, u32[]{:S(2)}, u32[]{:S(2)}) async-start(f16[32,40,128]{2,1,0:T(8,128)(2,1)} %convert_element_type.6), calls=%async_computation | async-start | bytes 655360 | tf_op jit(solution)/shard_map/all_to_all | solution.py:307
  21.5 0.0 copy-done
  21.5 0.1 collective-permute-start
  21.6 1.2 %collective-permute-done.pair = bf16[4,512]{1,0:T(4,128)(2,1)S(1)} collective-permute-done((bf16[4,512]{1,0:T(4,128)(2,1)S(1)}, bf16[4,512]{1,0:T(4,128)(2,1)S(1)}, u32[]{:S(2)}, u32[]{:S(2)}) %collective-permute-start) | collective-permute-done | bytes 4128 | tf_op jit(solution)/shard_map/ppermute | solution.py:289
  22.8 0.0 copy-start.1
  22.8 0.0 copy-start.2
  22.8 0.6 %collective-permute-start.1 = (bf16[2,4,512]{2,1,0:T(4,128)(2,1)S(1)}, bf16[2,4,512]{2,1,0:T(4,128)(2,1)S(1)}, u32[]{:S(2)}, u32[]{:S(2)}) collective-permute-start(bf16[2,4,512]{2,1,0:T(4,128)(2,1)S(1)} %pad_maximum_fusion), channel_id=1, source_target_pairs={{0,2},{1,3},{2,4},{3,5},{4,6},{5,7},{6,0},{7,1},{8,10},{9,11},{10,... | collective-permute-start | bytes 24584 | tf_op jit(solution)/shard_map/ppermute | solution.py:312
  23.4 2.4 %collective-permute-start.2 = (bf16[2,4,512]{2,1,0:T(4,128)(2,1)S(1)}, bf16[2,4,512]{2,1,0:T(4,128)(2,1)S(1)}, u32[]{:S(2)}, u32[]{:S(2)}) collective-permute-start(bf16[2,4,512]{2,1,0:T(4,128)(2,1)S(1)} %pad_maximum_fusion), channel_id=1, source_target_pairs={{0,4},{1,5},{2,6},{3,7},{4,0},{5,1},{6,2},{7,3},{8,12},{9,13},{10,... | collective-permute-start | bytes 24584 | tf_op jit(solution)/shard_map/ppermute | solution.py:312
  25.8 0.0 collective-permute-start.3
  25.8 1.7 %prepare.1 = (f32[2,4,256]{2,1,0:T(4,128)S(1)}, bf16[3,1024,256]{2,1,0:T(8,128)(2,1)S(1)}) custom-call(bf16[4,512]{1,0:T(4,128)(2,1)S(1)} %copy-done, bf16[4,512]{1,0:T(4,128)(2,1)S(1)} %collective-permute-done.pair, bf16[4096,256]{1,0:T(8,128)(2,1)} %forget_weight.3, bf16[4096,256]{1,0:T(8,128)(2,1)} %refs_5_.1), custom_call_target="tpu_custom_call" | custom-call | tf_op jit(solution)/shard_map/prepare/pallas_call | solution.py:315
  27.5 0.0 collective-permute-done.1.refs_0_
  27.5 1.0 %collective-permute-done.2.refs_1_ = bf16[2,4,512]{2,1,0:T(4,128)(2,1)S(1)} collective-permute-done((bf16[2,4,512]{2,1,0:T(4,128)(2,1)S(1)}, bf16[2,4,512]{2,1,0:T(4,128)(2,1)S(1)}, u32[]{:S(2)}, u32[]{:S(2)}) %collective-permute-start.2) | collective-permute-done | bytes 8224 | tf_op jit(solution)/shard_map/ppermute | solution.py:312
  28.5 2.1 %collective-permute-done.3.refs_2_ = bf16[2,4,512]{2,1,0:T(4,128)(2,1)S(1)} collective-permute-done((bf16[2,4,512]{2,1,0:T(4,128)(2,1)S(1)}, bf16[2,4,512]{2,1,0:T(4,128)(2,1)S(1)}, u32[]{:S(2)}, u32[]{:S(2)}) %collective-permute-start.3) | collective-permute-done | bytes 8224 | tf_op jit(solution)/shard_map/ppermute | solution.py:312
  30.7 0.0 copy-done.1
  30.7 0.0 copy-done.2
  30.7 0.0 copy-start.3
  30.7 2.3 %token_.1 = (f32[8,128]{1,0:T(8,128)S(1)}, f32[8,128]{1,0:T(8,128)S(1)}) custom-call(bf16[2,4,512]{2,1,0:T(4,128)(2,1)S(1)} %collective-permute-done.1.refs_0_, bf16[2,4,512]{2,1,0:T(4,128)(2,1)S(1)} %collective-permute-done.2.refs_1_, bf16[2,4,512]{2,1,0:T(4,128)(2,1)S(1)} %collective-permute-done.3.refs_2_, f32[2,4,256]{2,1,0:T(4,128)S(1)} %get-tuple-element.12.refs_3_, ...), custom_call_target="tpu_custom_call" | custom-call | tf_op jit(solution)/shard_map/token/pallas_call | solution.py:330
  33.0 2.6 %all-to-all-done = f16[32,40,128]{2,1,0:T(8,128)(2,1)S(1)} async-done(((f16[32,40,128]{2,1,0:T(8,128)(2,1)}), f16[32,40,128]{2,1,0:T(8,128)(2,1)S(1)}, u32[]{:S(2)}, u32[]{:S(2)}) %all-to-all-start) | async-done | bytes 327712 | tf_op jit(solution)/shard_map/all_to_all | solution.py:307
  35.6 1.0 %state.1 = (bf16[4,2,4,128]{3,2,1,0:T(4,128)(2,1)S(1)}, f32[32,8,128]{2,1,0:T(8,128)S(1)}) custom-call(f32[32,40,128]{2,1,0:T(8,128)S(1)} %convert_element_type.7.got, f32[8,128]{1,0:T(8,128)S(1)} %get-tuple-element.14.reach), custom_call_target="tpu_custom_call" | custom-call | tf_op jit(solution)/shard_map/state/pallas_call | solution.py:345
  36.7 17.5 %all_to_all.10.shares = f32[32,8,128]{2,1,0:T(8,128)S(1)} all-to-all(f32[32,8,128]{2,1,0:T(8,128)S(1)} %get-tuple-element.15), channel_id=1, replica_groups=mesh['sp'=32,'tp'=8] {'sp'}, dimensions={0} | all-to-all | bytes 262144 | tf_op jit(solution)/shard_map/all_to_all | solution.py:355
  54.2 0.0 copy-done.3
  54.2 0.7 %read.1 = (bf16[4,2,4,128]{3,2,1,0:T(4,128)(2,1)}, bf16[4,256]{1,0:T(4,128)(2,1)}) custom-call(f32[32,8,128]{2,1,0:T(8,128)S(1)} %all_to_all.10.shares, f32[8,128]{1,0:T(8,128)S(1)} %get-tuple-element.16.addend, f32[1,128]{1,0:T(1,128)S(1)} %bitcast.8, bf16[4,2,4,128]{3,2,1,0:T(4,128)(2,1)S(1)} %get-tuple-element.17.final), custom_call_target="tpu_custom_call" | custom-call | tf_op jit(solution)/shard_map/read/pallas_call | solution.py:356
  (2 shorter events, 0.1 us)
Async XLA Ops:
  0.6 20.9 %copy-start = (bf16[4,512]{1,0:T(4,128)(2,1)S(1)}, bf16[4,512]{1,0:T(4,128)(2,1)}, u32[]{:S(2)}) copy-start(bf16[4,512]{1,0:T(4,128)(2,1)} %own) | copy-start | bytes 12292
  10.0 25.6 %all-to-all-start = ((f16[32,40,128]{2,1,0:T(8,128)(2,1)}), f16[32,40,128]{2,1,0:T(8,128)(2,1)S(1)}, u32[]{:S(2)}, u32[]{:S(2)}) async-start(f16[32,40,128]{2,1,0:T(8,128)(2,1)} %convert_element_type.6), calls=%async_computation | async-start | bytes 655360 | tf_op jit(solution)/shard_map/all_to_all | solution.py:307
  21.5 1.3 %collective-permute-start = (bf16[4,512]{1,0:T(4,128)(2,1)S(1)}, bf16[4,512]{1,0:T(4,128)(2,1)S(1)}, u32[]{:S(2)}, u32[]{:S(2)}) collective-permute-start(bf16[4,512]{1,0:T(4,128)(2,1)S(1)} %copy-done), channel_id=1, source_target_pairs={{0,1},{1,0},{2,3},{3,2},{4,5},{5,4},{6,7},{7,6},{8,9},{9,8},{10,11... | collective-permute-start | bytes 12296 | tf_op jit(solution)/shard_map/ppermute | solution.py:289
  22.8 7.9 %copy-start.1 = (f32[256]{0:T(256)S(1)}, f32[256]{0:T(256)}, u32[]{:S(2)}) copy-start(f32[256]{0:T(256)} %param.11) | copy-start | bytes 3076
  22.8 7.9 %copy-start.2 = (bf16[4,256]{1,0:T(4,128)(2,1)S(1)}, bf16[4,256]{1,0:T(4,128)(2,1)}, u32[]{:S(2)}) copy-start(bf16[4,256]{1,0:T(4,128)(2,1)} %refs_7_.1) | copy-start | bytes 6148
  22.8 4.7 %collective-permute-start.1 = (bf16[2,4,512]{2,1,0:T(4,128)(2,1)S(1)}, bf16[2,4,512]{2,1,0:T(4,128)(2,1)S(1)}, u32[]{:S(2)}, u32[]{:S(2)}) collective-permute-start(bf16[2,4,512]{2,1,0:T(4,128)(2,1)S(1)} %pad_maximum_fusion), channel_id=1, source_target_pairs={{0,2},{1,3},{2,4},{3,5},{4,6},{5,7},{6,0},{7,1},{8,10},{9,11},{10,... | collective-permute-start | bytes 24584 | tf_op jit(solution)/shard_map/ppermute | solution.py:312
  23.4 5.2 %collective-permute-start.2 = (bf16[2,4,512]{2,1,0:T(4,128)(2,1)S(1)}, bf16[2,4,512]{2,1,0:T(4,128)(2,1)S(1)}, u32[]{:S(2)}, u32[]{:S(2)}) collective-permute-start(bf16[2,4,512]{2,1,0:T(4,128)(2,1)S(1)} %pad_maximum_fusion), channel_id=1, source_target_pairs={{0,4},{1,5},{2,6},{3,7},{4,0},{5,1},{6,2},{7,3},{8,12},{9,13},{10,... | collective-permute-start | bytes 24584 | tf_op jit(solution)/shard_map/ppermute | solution.py:312
  25.8 4.9 %collective-permute-start.3 = (bf16[2,4,512]{2,1,0:T(4,128)(2,1)S(1)}, bf16[2,4,512]{2,1,0:T(4,128)(2,1)S(1)}, u32[]{:S(2)}, u32[]{:S(2)}) collective-permute-start(bf16[2,4,512]{2,1,0:T(4,128)(2,1)S(1)} %pad_maximum_fusion), channel_id=1, source_target_pairs={{0,6},{1,7},{2,0},{3,1},{4,2},{5,3},{6,4},{7,5},{8,14},{9,15},{10,... | collective-permute-start | bytes 24584 | tf_op jit(solution)/shard_map/ppermute | solution.py:312
  30.7 23.5 %copy-start.3 = (f32[128]{0:T(128)S(1)}, f32[128]{0:T(128)}, u32[]{:S(2)}) copy-start(f32[128]{0:T(128)} %param.15) | copy-start | bytes 1540
